TPU v7x, 1024 devices: a whole 4x4x32 slice. The times are simulated.
1024 devices in a mesh: sp: 128 (over z, y), tp: 8 (over x, core).
Axes of the slice: x: 4, y: 4, z: 32, core: 2. Of those that a mesh axis runs over, the one named last changes fastest.
Arguments:
- query_rows: bfloat16 [32768, 2048], P('sp', 'tp'), may hold values from -5.5 to 5.5
- key_rows: bfloat16 [32768, 2048], P('sp', 'tp'), may hold values from -5.5 to 5.5
- value_rows: bfloat16 [32768, 2048], P('sp', 'tp'), may hold values from -6 to 6
- out_grad: bfloat16 [32768, 2048], P('sp', 'tp'), may hold values from -96 to 96
- rel_bias: float32 [256, 32], replicated, may hold values from -3 to 3
Outputs:
- query_grad: bfloat16 [32768, 2048], P('sp', 'tp')
- key_grad: bfloat16 [32768, 2048], P('sp', 'tp')
- value_grad: bfloat16 [32768, 2048], P('sp', 'tp')
- table_grad: float32 [256, 32], P('sp')
All inputs are finite; a program needn't handle non-finite values.
Results may differ from a plain program's by a relative error of at most 0.007.
Values may be sent and summed in bfloat16 or wider, within the bound.
No kernel may reach another device: no remote copies, remote signals or barrier semaphores. Data moves between devices by JAX's collectives and lax.ppermute only.
A program may use at most 32 MiB of HBM per device.

v0:
```python
from functools import partial

import jax
import jax.numpy as jnp
from jax import lax
from jax.sharding import Mesh
from jax.sharding import PartitionSpec as P

HEAD_DIM = 64
SEG = 64
LEFT = 4
CLIP = 128
SP = ("sp_0", "sp_1")


NEG_FILL = -1e30


def passed_along(block, axis, distance):
    devices = range(lax.axis_size(axis))
    route = [(i - distance, i) for i in devices if i - distance in devices]
    return lax.ppermute(block, axis, route)


def sum_by_axis(array, axes, dim):
    if not axes:
        return array
    nearer = lax.psum_scatter(array, axes[0], scatter_dimension=dim, tiled=True)
    return sum_by_axis(nearer, axes[1:], dim)


def in_order(pieces, dim):
    pieces = jnp.moveaxis(pieces, 0, dim)
    lengths = pieces.shape
    return pieces.reshape(*lengths[:dim], lengths[dim] * lengths[dim + 1], *lengths[dim + 2 :])


def copy_for_each(array, axis):
    copies = jnp.broadcast_to(array, (lax.axis_size(axis), *array.shape))
    return lax.all_to_all(copies, axis, split_axis=0, concat_axis=0, tiled=True)


def gathered_copies(array, axis, dim):
    return in_order(copy_for_each(array, axis), dim)


def banded(extended, seg_count, seg_len, band_len):
    layers = []
    for offset in range(band_len // seg_len):
        window = lax.slice_in_dim(
            extended, offset * seg_len, offset * seg_len + seg_count * seg_len, axis=0
        )
        layers.append(window.reshape((seg_count, 1, seg_len) + extended.shape[1:]))
    return jnp.concatenate(layers, axis=1).reshape((seg_count, band_len) + extended.shape[1:])


def unbanded(band_grads, ext_len, seg_len):
    seg_count, band_len = (band_grads.shape[0], band_grads.shape[1])
    trailing = band_grads.shape[2:]
    blocks = band_grads.reshape((seg_count, band_len // seg_len, seg_len) + trailing)
    summed = jnp.zeros((ext_len,) + trailing, band_grads.dtype)
    for offset in range(band_len // seg_len):
        stripe = blocks[:, offset].reshape((seg_count * seg_len,) + trailing)
        widths = [(offset * seg_len, ext_len - offset * seg_len - seg_count * seg_len)] + [
            (0, 0)
        ] * len(trailing)
        summed = summed + jnp.pad(stripe, widths)
    return summed


def diagonal_sums(square, rel_top, table_rows, clip_half):
    row_count, col_count = square.shape
    flipped = square[::-1]
    padded = jnp.pad(flipped, ((0, 0), (0, row_count)))
    sheared = padded.reshape(-1)[: row_count * (col_count + row_count - 1)].reshape(
        row_count, col_count + row_count - 1
    )
    diagonals = jnp.sum(sheared, axis=0)
    relative = rel_top - jnp.arange(col_count + row_count - 1, dtype=jnp.int32)
    bin_index = jnp.clip(relative, -clip_half, clip_half - 1) + clip_half
    onehot = bin_index[:, None] == jnp.arange(table_rows, dtype=jnp.int32)[None, :]
    return jnp.sum(jnp.where(onehot, diagonals[:, None], 0.0), axis=0)


def segment_grads(query_segs, dout_segs, key_ext, value_ext, key_valid, bias_band):
    seg_len, band_len = bias_band.shape
    seg_count = query_segs.shape[0]
    score_scale = query_segs.shape[-1] ** (-0.5)
    key_band = banded(key_ext, seg_count, seg_len, band_len)
    value_band = banded(value_ext, seg_count, seg_len, band_len)
    valid_band = banded(key_valid, seg_count, seg_len, band_len)
    scores = (
        jnp.einsum("jid,jcd->jic", query_segs, key_band, preferred_element_type=jnp.float32)
        * score_scale
        + bias_band[None]
    )
    scores = jnp.where(valid_band[:, None, :], scores, NEG_FILL)
    row_peak = jnp.max(scores, axis=-1)
    log_norm = row_peak + jnp.log(jnp.sum(jnp.exp(scores - row_peak[..., None]), axis=-1))
    attention = jnp.exp(scores - log_norm[..., None])
    attention_half = attention.astype(jnp.bfloat16)
    attention_grad = jnp.einsum(
        "jie,jce->jic", dout_segs, value_band, preferred_element_type=jnp.float32
    )
    inner_sums = jnp.sum(attention * attention_grad, axis=-1)
    dscores = attention * (attention_grad - inner_sums[..., None])
    dscore_half = dscores.astype(jnp.bfloat16)
    dquery = (
        jnp.einsum("jic,jcd->jid", dscore_half, key_band, preferred_element_type=jnp.float32)
        * score_scale
    )
    dkey_band = (
        jnp.einsum("jic,jid->jcd", dscore_half, query_segs, preferred_element_type=jnp.float32)
        * score_scale
    )
    dvalue_band = jnp.einsum(
        "jic,jie->jce", attention_half, dout_segs, preferred_element_type=jnp.float32
    )
    ext_len = key_ext.shape[0]
    return (
        dquery,
        unbanded(dkey_band, ext_len, seg_len),
        unbanded(dvalue_band, ext_len, seg_len),
        jnp.sum(dscores, axis=0),
        log_norm,
        inner_sums,
    )


def by_heads(row_block):
    return jnp.transpose(
        row_block.reshape(row_block.shape[0], row_block.shape[1] // HEAD_DIM, HEAD_DIM), (1, 0, 2)
    )


def from_heads(stacked):
    return jnp.transpose(stacked, (1, 0, 2)).reshape(
        stacked.shape[1], stacked.shape[0] * stacked.shape[2]
    )


def shards(query_rows, key_rows, value_rows, out_grad, rel_bias):
    tok_rows, width_here = query_rows.shape
    heads_here = width_here // HEAD_DIM
    reach_rows = LEFT * SEG
    band_len = reach_rows + SEG
    seg_count = tok_rows // SEG
    distance = 1
    received = [passed_along((key_rows, value_rows), SP, distance)]
    halo_keys = jnp.concatenate([arrived[0] for arrived in received], axis=0)
    halo_values = jnp.concatenate([arrived[1] for arrived in received], axis=0)
    key_ext = jnp.concatenate([halo_keys, key_rows], axis=0)
    value_ext = jnp.concatenate([halo_values, value_rows], axis=0)
    first_row = lax.axis_index(SP) * tok_rows - reach_rows
    key_valid = first_row + jnp.arange(reach_rows + tok_rows, dtype=jnp.int32) >= 0
    table_here = lax.dynamic_slice_in_dim(
        rel_bias, lax.axis_index("tp") * heads_here, heads_here, 1
    )
    row_pos = jnp.arange(SEG, dtype=jnp.int32)[:, None]
    col_pos = jnp.arange(band_len, dtype=jnp.int32)[None, :]
    offset_index = jnp.clip(reach_rows + row_pos - col_pos, -CLIP, CLIP - 1) + CLIP
    bias_bands = jnp.transpose(jnp.take(table_here, offset_index, axis=0), (2, 0, 1))

    def own_head(inputs):
        query_head, dout_head, key_head, value_head, bias_band = inputs
        return segment_grads(
            query_head.reshape(seg_count, SEG, HEAD_DIM),
            dout_head.reshape(seg_count, SEG, HEAD_DIM),
            key_head,
            value_head,
            key_valid,
            bias_band,
        )

    dquery, dkey_ext, dvalue_ext, squares, log_norm, inner_sums = lax.map(
        own_head,
        (
            by_heads(query_rows),
            by_heads(out_grad),
            by_heads(key_ext),
            by_heads(value_ext),
            bias_bands,
        ),
    )
    query_grad = from_heads(dquery.reshape(heads_here, tok_rows, HEAD_DIM)).astype(jnp.bfloat16)
    key_total = from_heads(dkey_ext[:, reach_rows:])
    value_total = from_heads(dvalue_ext[:, reach_rows:])
    table_terms = jnp.transpose(
        jax.vmap(
            partial(
                diagonal_sums, rel_top=reach_rows + SEG - 1, table_rows=2 * CLIP, clip_half=CLIP
            )
        )(squares)
    )
    back_keys = from_heads(dkey_ext[:, :reach_rows])
    back_values = from_heads(dvalue_ext[:, :reach_rows])
    distance = 1
    arrived = (
        passed_along(back_keys.astype(jnp.bfloat16), SP, -distance).astype(back_keys.dtype),
        passed_along(back_values.astype(jnp.bfloat16), SP, -distance).astype(back_values.dtype),
    )
    key_total = key_total + arrived[0]
    value_total = value_total + arrived[1]
    partial_rows = sum_by_axis(table_terms, SP, 0)
    table_grad = gathered_copies(partial_rows, "tp", 1)
    return (
        query_grad,
        key_total.astype(jnp.bfloat16),
        value_total.astype(jnp.bfloat16),
        table_grad,
    )


def solution(mesh):
    finer = Mesh(mesh.devices.reshape(32, 4, mesh.shape["tp"]), ("sp_0", "sp_1", "tp"))
    return jax.shard_map(
        shards,
        mesh=finer,
        in_specs=(P(SP, "tp"), P(SP, "tp"), P(SP, "tp"), P(SP, "tp"), P()),
        out_specs=(P(SP, "tp"), P(SP, "tp"), P(SP, "tp"), P(SP, None)),
        check_vma=False,
    )
```

profile of v0, /device:TPU:1, one launch (start us, length us, event | category | flops | bytes accessed | tf_op | source)
XLA Modules:
  0.0 272.8 jit_solution(13195695274241559743)
XLA Ops:
  0.6 1.0 copy.170
  1.7 4.0 %collective-permute-start = (bf16[256,256]{0,1:T(8,128)(2,1)S(1)}, bf16[256,256]{0,1:T(8,128)(2,1)S(1)}, u32[]{:S(2)}, u32[]{:S(2)}) collective-permute-start(bf16[256,256]{0,1:T(8,128)(2,1)S(1)} %copy.170), channel_id=1, source_target_pairs={{0,8},{8,16},{16,24},{24,32},{32,40},{40,48},{48,56},{56,64},{64,7... | collective-permute-start | bytes 393224 | tf_op jit(solution)/shard_map/ppermute | solution.py:22
  5.7 1.0 copy.175
  6.7 3.2 %collective-permute-start.1 = (bf16[256,256]{0,1:T(8,128)(2,1)S(1)}, bf16[256,256]{0,1:T(8,128)(2,1)S(1)}, u32[]{:S(2)}, u32[]{:S(2)}) collective-permute-start(bf16[256,256]{0,1:T(8,128)(2,1)S(1)} %copy.175), channel_id=1, source_target_pairs={{0,8},{8,16},{16,24},{24,32},{32,40},{40,48},{48,56},{56,64},{64,7... | collective-permute-start | bytes 393224 | tf_op jit(solution)/shard_map/ppermute | solution.py:22
  10.5 68.0 %gather_fusion = f32[20480,4]{1,0:T(8,128)} fusion(f32[256,4]{1,0:T(8,128)S(1)} %copy.207, s32[20480]{0:T(1024)S(1)} %broadcast_clamp_fusion), kind=kCustom, calls=%fused_computation | custom fusion | bytes 737280 | tf_op jit(solution)/shard_map/jit(_take)/gather | solution.py:162
  78.5 6.5 %copy.173 = f32[64,320,4]{1,0,2:T(8,128)S(1)} copy(f32[64,320,4]{2,1,0:T(8,128)} %bitcast.236) | data formatting | bytes 655360 | tf_op jit(solution)/shard_map/jit(_take)/gather | solution.py:162
  85.6 1.3 dynamic-slice
  86.9 1.3 dynamic-slice.2
  89.5 26.0 %while.19 = (s32[]{:T(128)}, bf16[4,4,64,64]{3,2,1,0:T(8,128)(2,1)}, f32[4,512,64]{1,2,0:T(8,128)}, f32[4,512,64]{1,2,0:T(8,128)}, f32[4,64,320]{2,1,0:T(8,128)}...) while((s32[]{:T(128)}, ...), condition=%wide.wide.region_5.6_spmd, body=%wide.wide.region_0.5_spmd.sunk | while | flops 54078980 | bytes 11466761 | solution.py:175
  92.0 0.3 multiply_reduce_fusion.3
  93.2 0.4 fusion.73
  93.8 0.7 constant_dynamic-update-slice_fusion.44
  94.5 0.7 bitcast_dynamic-update-slice_fusion.3
  95.2 0.8 fusion.72
  98.4 0.3 multiply_reduce_fusion.3
  99.7 0.4 fusion.73
  100.3 0.7 constant_dynamic-update-slice_fusion.44
  101.0 0.6 bitcast_dynamic-update-slice_fusion.3
  101.7 0.8 fusion.72
  104.9 0.3 multiply_reduce_fusion.3
  106.2 0.4 fusion.73
  106.8 0.7 constant_dynamic-update-slice_fusion.44
  107.5 0.6 bitcast_dynamic-update-slice_fusion.3
  108.2 0.8 fusion.72
  111.4 0.3 multiply_reduce_fusion.3
  112.6 0.4 fusion.73
  113.3 0.7 constant_dynamic-update-slice_fusion.44
  114.0 0.6 bitcast_dynamic-update-slice_fusion.3
  114.7 0.8 fusion.72
  115.5 1.0 slice.219
  116.5 1.0 slice.194
  117.4 1.0 slice.220
  118.4 1.0 slice.192
  119.4 1.3 collective-permute-start.3
  120.7 1.3 collective-permute-start.2
  122.0 1.8 rev.3
  124.1 0.4 reshape.302
  124.8 0.6 select_reduce_fusion
  125.5 96.7 %all-reduce.11 = f32[256,4]{1,0:T(8,128)S(1)} all-reduce(f32[256,4]{1,0:T(8,128)S(1)} %copy.187), channel_id=2, replica_groups=mesh['sp_0'=32,'sp_1'=4,'tp'=8] {'sp_0'}, use_global_device_ids=true, to_apply=%region_8.9.clone | all-reduce | flops 1024 | bytes 8192
  222.2 7.3 %all-reduce.12 = f32[8,4]{1,0:T(8,128)S(1)} all-reduce(f32[8,4]{1,0:T(8,128)S(1)} %constant_dynamic-slice_fusion.13), channel_id=3, replica_groups=mesh['sp_0'=32,'sp_1'=4,'tp'=8] {'sp_1'}, use_global_device_ids=true, to_apply=%region_9.10.clone | all-reduce | flops 32 | bytes 256
  229.5 0.6 broadcast_in_dim.101
  230.1 35.8 %all-to-all-start = ((f32[8,2,4]{2,1,0:T(2,128)}), f32[8,2,4]{2,1,0:T(2,128)S(1)}, u32[]{:S(2)}, u32[]{:S(2)}) async-start(f32[8,2,4]{2,1,0:T(2,128)} %broadcast_in_dim.101), calls=%async_computation | async-start | bytes 16384 | tf_op jit(solution)/shard_map/all_to_all | solution.py:40
  265.9 1.1 copy.198
  267.0 0.8 copy.189
  267.8 2.8 %all-to-all-done = f32[8,2,4]{2,1,0:T(2,128)S(1)} async-done(((f32[8,2,4]{2,1,0:T(2,128)}), f32[8,2,4]{2,1,0:T(2,128)S(1)}, u32[]{:S(2)}, u32[]{:S(2)}) %all-to-all-start) | async-done | bytes 288 | tf_op jit(solution)/shard_map/all_to_all | solution.py:40
  270.6 0.6 reshape.303
  271.2 0.8 copy.191
  272.0 0.8 copy.190
  (200 shorter events, 15.2 us)
Async XLA Ops:
  0.6 9.6 %copy-start = (f32[256,32]{0,1:T(8,128)S(1)}, f32[256,32]{0,1:T(8,128)}, u32[]{:S(2)}) copy-start(f32[256,32]{0,1:T(8,128)} %param.11) | copy-start | bytes 98308
  1.7 87.8 %collective-permute-start = (bf16[256,256]{0,1:T(8,128)(2,1)S(1)}, bf16[256,256]{0,1:T(8,128)(2,1)S(1)}, u32[]{:S(2)}, u32[]{:S(2)}) collective-permute-start(bf16[256,256]{0,1:T(8,128)(2,1)S(1)} %copy.170), channel_id=1, source_target_pairs={{0,8},{8,16},{16,24},{24,32},{32,40},{40,48},{48,56},{56,64},{64,7... | collective-permute-start | bytes 393224 | tf_op jit(solution)/shard_map/ppermute | solution.py:22
  6.7 82.8 %collective-permute-start.1 = (bf16[256,256]{0,1:T(8,128)(2,1)S(1)}, bf16[256,256]{0,1:T(8,128)(2,1)S(1)}, u32[]{:S(2)}, u32[]{:S(2)}) collective-permute-start(bf16[256,256]{0,1:T(8,128)(2,1)S(1)} %copy.175), channel_id=1, source_target_pairs={{0,8},{8,16},{16,24},{24,32},{32,40},{40,48},{48,56},{56,64},{64,7... | collective-permute-start | bytes 393224 | tf_op jit(solution)/shard_map/ppermute | solution.py:22
  78.5 6.9 %copy-start.1 = (bf16[256,256]{1,0:T(8,128)(2,1)S(1)}, bf16[256,256]{1,0:T(8,128)(2,1)}, u32[]{:S(2)}) copy-start(bf16[256,256]{1,0:T(8,128)(2,1)} %param.7) | copy-start | bytes 393220
  78.5 7.0 %copy-start.2 = (bf16[256,256]{1,0:T(8,128)(2,1)S(1)}, bf16[256,256]{1,0:T(8,128)(2,1)}, u32[]{:S(2)}) copy-start(bf16[256,256]{1,0:T(8,128)(2,1)} %param.10) | copy-start | bytes 393220
  85.3 4.2 %copy-start.3 = (pred[4,5,64]{2,1,0:T(8,128)(4,1)}, pred[4,5,64]{2,1,0:T(8,128)(4,1)S(1)}, u32[]{:S(2)}) copy-start(pred[4,5,64]{2,1,0:T(8,128)(4,1)S(1)} %concatenate.23) | copy-start | bytes 3844
  119.4 151.8 %collective-permute-start.3 = (bf16[256,256]{0,1:T(8,128)(2,1)S(1)}, bf16[256,256]{0,1:T(8,128)(2,1)S(1)}, u32[]{:S(2)}, u32[]{:S(2)}) collective-permute-start(bf16[256,256]{0,1:T(8,128)(2,1)S(1)} %bitcast.272), channel_id=1, source_target_pairs={{8,0},{16,8},{24,16},{32,24},{40,32},{48,40},{56,48},{64,56},{72,6... | collective-permute-start | bytes 393224 | tf_op jit(solution)/shard_map/ppermute | solution.py:22
  120.7 151.3 %collective-permute-start.2 = (bf16[256,256]{0,1:T(8,128)(2,1)S(1)}, bf16[256,256]{0,1:T(8,128)(2,1)S(1)}, u32[]{:S(2)}, u32[]{:S(2)}) collective-permute-start(bf16[256,256]{0,1:T(8,128)(2,1)S(1)} %bitcast.271), channel_id=1, source_target_pairs={{8,0},{16,8},{24,16},{32,24},{40,32},{48,40},{56,48},{64,56},{72,6... | collective-permute-start | bytes 393224 | tf_op jit(solution)/shard_map/ppermute | solution.py:22
  230.1 40.4 %all-to-all-start = ((f32[8,2,4]{2,1,0:T(2,128)}), f32[8,2,4]{2,1,0:T(2,128)S(1)}, u32[]{:S(2)}, u32[]{:S(2)}) async-start(f32[8,2,4]{2,1,0:T(2,128)} %broadcast_in_dim.101), calls=%async_computation | async-start | bytes 16384 | tf_op jit(solution)/shard_map/all_to_all | solution.py:40
where the time goes:
time: 273 us
  local copies, waits for them, and re-layouts  106 us (39%)
  blocking collectives  104 us (38%)
  starting transfers between devices  45.6 us (17%)
  matrix products  8.42 us (3%)
  other arithmetic  3.09 us (1%)
  waiting for transfers between devices  2.8 us (1%)
    unnamed x2, blocking collectives  104 us
    gather x2, local copies, waits for them, and re-layouts, shards(): jnp.take(table_here, offset_index, axis=0)  74.5 us
    all_to_all x1, starting transfers between devices, copy_for_each(): return lax.all_to_all(copies, axis, split_axis=0, concat_axis=0, tiled=True)  35.8 us
    ppermute x4, starting transfers between devices, passed_along(): return lax.ppermute(block, axis, route)  9.81 us
    unnamed x22, local copies, waits for them, and re-layouts  7.48 us
    dynamic_update_slice x16, local copies, waits for them, and re-layouts, shards(): lax.map(own_head, (by_heads(query_rows), by_heads(out_grad), by_heads(key...  6.39 us
  transfers between devices with their start and end apart: 5, of which 1 were waited for; matrix products, arithmetic and copies ran while one was open for 32% of the time, Pallas kernels for 0%

commit v1 on v0

v1 whole, which is shorter than its diff:
```python
from functools import partial

import jax
import jax.numpy as jnp
from jax import lax
from jax.experimental import pallas as pl
from jax.experimental.pallas import tpu as pltpu
from jax.sharding import PartitionSpec as P

HEAD_DIM = 64
SEG = 64
LEFT = 4
CLIP = 128
NEG_FILL = -1e30
HIGHEST = lax.Precision.HIGHEST

REACH = LEFT * SEG
PAIR = 2 * SEG
WIN = REACH + PAIR

NT = (((1,), (1,)), ((), ()))
TN = (((0,), (0,)), ((), ()))
NN = (((1,), (0,)), ((), ()))


def dot(a, b, dims, **kw):
    return lax.dot_general(a, b, dims, preferred_element_type=jnp.float32, **kw)


def bias_kernel(first_head, table_ref, bias_ref):
    heads = bias_ref.shape[1] // PAIR
    wide = table_ref.shape[1]
    start = first_head(heads)
    pick = lax.broadcasted_iota(jnp.int32, (8, wide), 1) == lax.broadcasted_iota(jnp.int32, (8, wide), 0) + start
    rows = dot(jnp.where(pick, 1.0, 0.0), table_ref[...], NT, precision=HIGHEST)
    key_of = lax.broadcasted_iota(jnp.int32, (PAIR, PAIR), 0)
    query_of = lax.broadcasted_iota(jnp.int32, (PAIR, PAIR), 1)
    early = query_of < SEG
    low = key_of < SEG
    after = query_of >= key_of
    for head in range(heads):
        lanes = slice(head * PAIR, (head + 1) * PAIR)
        neg = jnp.broadcast_to(rows[head : head + 1, :CLIP], (PAIR, PAIR))
        pos = jnp.broadcast_to(rows[head : head + 1, CLIP:], (PAIR, PAIR))
        neg = pltpu.roll(neg, 0, 1, stride=1, stride_axis=0)
        pos = pltpu.roll(pos, 0, 1, stride=1, stride_axis=0)
        top = rows[head : head + 1, 2 * CLIP - 1 :]
        bias_ref[0:PAIR, lanes] = jnp.where(low & ~early, NEG_FILL, jnp.broadcast_to(top, (PAIR, PAIR)))
        bias_ref[PAIR : 2 * PAIR, lanes] = jnp.where(after, top, pos)
        bias_ref[2 * PAIR : 3 * PAIR, lanes] = jnp.where(early & ~low, NEG_FILL, jnp.where(after, pos, neg))


def diagonals(squares):
    rows = PAIR
    while rows > 8:
        half = rows // 2
        squares = [s[:half] + pltpu.roll(s[half:], PAIR - half, 1) for s in squares]
        rows = half
    row_of = lax.broadcasted_iota(jnp.int32, (8, PAIR), 0)
    sums = []
    for s in squares:
        for bit in (4, 2, 1):
            s = jnp.where((row_of & bit) != 0, pltpu.roll(s, PAIR - bit, 1), s)
        sums.append(jnp.sum(s, axis=0, keepdims=True))
    return sums


def grads_kernel(
    first_head,
    is_first,
    query_ref,
    key_ref,
    value_ref,
    dout_ref,
    halo_key_ref,
    halo_value_ref,
    bias_ref,
    dquery_ref,
    dkey_ref,
    dvalue_ref,
    back_key_ref,
    back_value_ref,
    table_ref,
):
    rows, width = query_ref.shape
    heads = width // HEAD_DIM
    scale = HEAD_DIM**-0.5
    lane_head = lax.broadcasted_iota(jnp.int32, (PAIR, width), 1) // HEAD_DIM
    halo_fill = jnp.where(is_first(), NEG_FILL, 0.0)

    def by_head(block):
        zero = jnp.zeros_like(block)
        return jnp.concatenate([jnp.where(lane_head == h, block, zero) for h in range(heads)], axis=0)

    def window(halo_ref, own_ref, start):
        parts = []
        if start < REACH:
            parts.append(halo_ref[start:REACH, :])
        stop = start + WIN - REACH
        parts.append(own_ref[max(start - REACH, 0) : stop, :])
        return jnp.concatenate(parts, axis=0)

    dscore_sum = None
    for pair in range(rows // PAIR):
        start = pair * PAIR
        halo_rows = max(REACH - start, 0)
        query = by_head(query_ref[start : start + PAIR, :])
        dout = by_head(dout_ref[start : start + PAIR, :])
        keys = window(halo_key_ref, key_ref, start)
        values = window(halo_value_ref, value_ref, start)
        scores = dot(keys, query, NT) * scale + bias_ref[...]
        if halo_rows:
            scores = jnp.concatenate([scores[:halo_rows] + halo_fill, scores[halo_rows:]], axis=0)
        peak = jnp.max(scores, axis=0, keepdims=True)
        weights = jnp.exp(scores - peak)
        total = jnp.sum(weights, axis=0, keepdims=True)
        probs = weights * (1.0 / total)
        dprobs = dot(values, dout, NT)
        inner = jnp.sum(probs * dprobs, axis=0, keepdims=True)
        dscores = probs * (dprobs - inner)
        dscore_sum = dscores if dscore_sum is None else dscore_sum + dscores
        prob_half = probs.astype(jnp.bfloat16)
        dscore_half = dscores.astype(jnp.bfloat16)
        dvalue = dot(prob_half, dout, NN)
        dkey = dot(dscore_half, query, NN) * scale
        stacked = dot(dscore_half, keys, TN) * scale
        dquery = stacked[:PAIR]
        for h in range(1, heads):
            dquery = jnp.where(lane_head == h, stacked[h * PAIR : (h + 1) * PAIR], dquery)
        dquery_ref[start : start + PAIR, :] = dquery.astype(jnp.bfloat16)
        if pair == 0:
            back_key_ref[...] = dkey[:REACH].astype(jnp.bfloat16)
            back_value_ref[...] = dvalue[:REACH].astype(jnp.bfloat16)
            held_key = dkey[PAIR:REACH]
            held_value = dvalue[PAIR:REACH]
            dkey_ref[0:PAIR, :] = dkey[REACH:]
            dvalue_ref[0:PAIR, :] = dvalue[REACH:]
        else:
            back_key_ref[PAIR:REACH, :] = (held_key + dkey[:PAIR]).astype(jnp.bfloat16)
            back_value_ref[PAIR:REACH, :] = (held_value + dvalue[:PAIR]).astype(jnp.bfloat16)
            dkey_ref[0:PAIR, :] += dkey[PAIR:REACH]
            dvalue_ref[0:PAIR, :] += dvalue[PAIR:REACH]
            dkey_ref[PAIR:, :] = dkey[REACH:]
            dvalue_ref[PAIR:, :] = dvalue[REACH:]

    key_of = lax.broadcasted_iota(jnp.int32, (PAIR, PAIR), 0)
    query_of = lax.broadcasted_iota(jnp.int32, (PAIR, PAIR), 1)
    after = query_of >= key_of
    squares, tops = [], []
    for h in range(heads):
        lanes = slice(h * PAIR, (h + 1) * PAIR)
        far, middle, near = (dscore_sum[b * PAIR : (b + 1) * PAIR, lanes] for b in range(3))
        squares.append(jnp.where(after, 0.0, near))
        squares.append(jnp.where(after, near, middle))
        tops.append(jnp.sum(far + jnp.where(after, middle, 0.0), axis=0, keepdims=True))
    sums = diagonals(squares)
    last = lax.broadcasted_iota(jnp.int32, (1, PAIR), 1) == PAIR - 1
    pad = [jnp.zeros((8 - heads, PAIR), jnp.float32)]
    neg = jnp.concatenate(sums[0::2] + pad, axis=0)
    pos = jnp.concatenate(
        [s + jnp.where(last, jnp.sum(t, axis=1, keepdims=True), 0.0) for s, t in zip(sums[1::2], tops)] + pad, axis=0
    )
    place = lax.broadcasted_iota(jnp.int32, (8, PAIR), 1) == lax.broadcasted_iota(jnp.int32, (8, PAIR), 0) + first_head(heads)
    place = jnp.where(place & (lax.broadcasted_iota(jnp.int32, (8, PAIR), 0) < heads), 1.0, 0.0)
    table_ref[0:CLIP, :] = dot(neg, place, TN, precision=HIGHEST)
    table_ref[CLIP:, :] = dot(pos, place, TN, precision=HIGHEST)


def first_head(heads):
    return lax.axis_index("tp") * heads


def is_first():
    return lax.axis_index("sp") == 0


def passed_along(block, distance):
    devices = range(lax.axis_size("sp"))
    return lax.ppermute(block, "sp", [(i - distance, i) for i in devices if i - distance in devices])


def shards(query_rows, key_rows, value_rows, out_grad, rel_bias):
    rows, width = query_rows.shape
    heads = width // HEAD_DIM
    table_rows, all_heads = rel_bias.shape
    ranks = lax.axis_size("sp")
    share = table_rows // ranks
    halo_keys = passed_along(key_rows, 1)
    halo_values = passed_along(value_rows, 1)
    bias = pl.pallas_call(
        partial(bias_kernel, first_head),
        out_shape=jax.ShapeDtypeStruct((WIN, heads * PAIR), jnp.float32),
        cost_estimate=pl.CostEstimate(flops=8_000_000_000, bytes_accessed=2_000_000, transcendentals=0),
        compiler_params=pltpu.CompilerParams(vmem_limit_bytes=8 << 20),
        name="bias_tile",
    )(rel_bias)
    half = jax.ShapeDtypeStruct((rows, width), jnp.bfloat16)
    full = jax.ShapeDtypeStruct((rows, width), jnp.float32)
    query_grad, key_own, value_own, back_keys, back_values, table = pl.pallas_call(
        partial(grads_kernel, first_head, is_first),
        out_shape=(half, full, full, half, half, jax.ShapeDtypeStruct((table_rows, PAIR), jnp.float32)),
        cost_estimate=pl.CostEstimate(flops=8_000_000_000, bytes_accessed=4_000_000, transcendentals=0),
        compiler_params=pltpu.CompilerParams(vmem_limit_bytes=24 << 20),
        name="segment_grads",
    )(query_rows, key_rows, value_rows, out_grad, halo_keys, halo_values, bias)
    key_grad = (key_own + passed_along(back_keys, -1)).astype(jnp.bfloat16)
    value_grad = (value_own + passed_along(back_values, -1)).astype(jnp.bfloat16)
    terms = lax.all_to_all(table.reshape(ranks, share, PAIR), "sp", 0, 0, tiled=True)
    mine = jnp.sum(terms, axis=0)
    groups = lax.axis_size("tp")
    copies = lax.all_to_all(jnp.broadcast_to(mine, (groups, share, PAIR)), "tp", 0, 0, tiled=True)
    table_grad = jnp.sum(copies, axis=0)[:, :all_heads]
    return query_grad, key_grad, value_grad, table_grad


def solution(mesh):
    return jax.shard_map(
        shards,
        mesh=mesh,
        in_specs=(P("sp", "tp"), P("sp", "tp"), P("sp", "tp"), P("sp", "tp"), P()),
        out_specs=(P("sp", "tp"), P("sp", "tp"), P("sp", "tp"), P("sp", None)),
        check_vma=False,
    )
```

time: 273 us -> 89.1 us (0.33)
  local copies, waits for them, and re-layouts: 106 us -> 1.48 us
  blocking collectives: 104 us -> 0 us
  waiting for transfers between devices: 2.8 us -> 25.8 us
  starting transfers between devices: 45.6 us -> 55 us
  matrix products: 8.42 us -> 0 us
  Pallas kernels: 0 us -> 3.71 us
    unnamed x2 -> x0, blocking collectives: 104 us -> none
    gather x2 -> x0, local copies, waits for them, and re-layouts: 74.5 us -> none  [shards(): jnp.take(table_here, offset_index, axis=0)]
    all_to_all x1 -> x2, waiting for transfers between devices: 2.78 us -> 21.4 us  [the longest x1 17.5 us: shards(): lax.all_to_all(table.reshape(ranks, share, PAIR), 'sp', 0, 0, tiled=True)]
    all_to_all x1 -> x2, starting transfers between devices: 35.8 us -> 45.1 us  [the longest x1 34.1 us: shards(): lax.all_to_all(table.reshape(ranks, share, PAIR), 'sp', 0, 0, tiled=True)]
    dot_general x20 -> x0, matrix products: 8.42 us -> none  [the longest x4 3.29 us: segment_grads(): jnp.einsum('jic,jcd->jid', dscore_half, key_band, preferred_element_type=...]
    unnamed x22 -> x9, local copies, waits for them, and re-layouts: 7.48 us -> 0.88 us
    dynamic_update_slice x16 -> x0, local copies, waits for them, and re-layouts: 6.39 us -> none  [shards(): lax.map(own_head, (by_heads(query_rows), by_heads(out_grad), by_heads(key...]
    slice x21 -> x0, local copies, waits for them, and re-layouts: 5.15 us -> none  [the longest x1 0.97 us: shards(): value_total = from_heads(dvalue_ext[:, reach_rows:])]
  transfers between devices with their start and end apart: 5 -> 6, of which waited for: 1 -> 4; matrix products, arithmetic and copies ran while one was open for 32% -> 3% of each run, Pallas kernels for 0% -> 1%
where the time goes in v1:
time: 89.1 us; the launch traced here: 88.7 us
  starting transfers between devices  55 us (62%)
  waiting for transfers between devices  25.8 us (29%)
  Pallas kernels  3.71 us (4%)
  other arithmetic  2.09 us (2%)
  local copies, waits for them, and re-layouts  1.48 us (2%)
    all_to_all x1, starting transfers between devices, shards(): lax.all_to_all(table.reshape(ranks, share, PAIR), 'sp', 0, 0, tiled=True)  34.1 us
    all_to_all x1, waiting for transfers between devices, shards(): lax.all_to_all(table.reshape(ranks, share, PAIR), 'sp', 0, 0, tiled=True)  17.5 us
    all_to_all x1, starting transfers between devices, shards(): lax.all_to_all(jnp.broadcast_to(mine, (groups, share, PAIR)), 'tp', 0, 0,...  11 us
    ppermute x4, starting transfers between devices, passed_along(): lax.ppermute(block, 'sp', [(i - distance, i) for i in devices if i - dist...  9.82 us
    ppermute x4, waiting for transfers between devices, passed_along(): lax.ppermute(block, 'sp', [(i - distance, i) for i in devices if i - dist...  4.36 us
    all_to_all x1, waiting for transfers between devices, shards(): lax.all_to_all(jnp.broadcast_to(mine, (groups, share, PAIR)), 'tp', 0, 0,...  3.93 us
    pallas_call x1, Pallas kernels, shards(): pl.pallas_call(partial(grads_kernel, first_head, is_first), out_shape=(ha...  3.23 us
  transfers between devices with their start and end apart: 6, of which 4 were waited for; matrix products, arithmetic and copies ran while one was open for 3% of the time, Pallas kernels for 1%

profile of v1, /device:TPU:1, one launch (start us, length us, event | category | flops | bytes accessed | tf_op | source)
XLA Modules:
  0.0 88.7 jit_solution(17720684457042872064)
XLA Ops:
  0.6 4.0 %collective-permute-start = (bf16[256,256]{1,0:T(8,128)(2,1)}, bf16[256,256]{1,0:T(8,128)(2,1)S(1)}, u32[]{:S(2)}, u32[]{:S(2)}) collective-permute-start(bf16[256,256]{1,0:T(8,128)(2,1)} %key_ref.1), channel_id=1, source_target_pairs={{0,8},{8,16},{16,24},{24,32},{32,40},{40,48},{48,56},{56,64},{64,7... | collective-permute-start | bytes 393224 | tf_op jit(solution)/shard_map/ppermute | solution.py:179
  4.7 3.2 %collective-permute-start.1 = (bf16[256,256]{1,0:T(8,128)(2,1)}, bf16[256,256]{1,0:T(8,128)(2,1)S(1)}, u32[]{:S(2)}, u32[]{:S(2)}) collective-permute-start(bf16[256,256]{1,0:T(8,128)(2,1)} %value_ref.1), channel_id=1, source_target_pairs={{0,8},{8,16},{16,24},{24,32},{32,40},{40,48},{48,56},{56,64},{64,7... | collective-permute-start | bytes 393224 | tf_op jit(solution)/shard_map/ppermute | solution.py:179
  7.9 0.9 copy.11.table_ref
  8.7 0.0 copy-start
  8.7 0.0 copy-start.1
  8.8 0.0 copy-start.2
  8.8 0.0 copy-start.3
  8.8 0.5 bias_tile.1.bias_ref
  9.3 0.0 collective-permute-done.halo_key_ref
  9.3 0.8 collective-permute-done.1.halo_value_ref
  10.1 0.0 copy-done
  10.1 0.0 copy-done.1
  10.1 0.0 copy-done.2
  10.1 0.0 copy-done.3
  10.1 3.2 %segment_grads.1 = (bf16[256,256]{1,0:T(8,128)(2,1)}, f32[256,256]{1,0:T(8,128)S(1)}, f32[256,256]{1,0:T(8,128)S(1)}, bf16[256,256]{1,0:T(8,128)(2,1)S(1)}, bf16...) custom-call(bf16[256,256]{1,0:T(8,128)(2,1)S(1)} %copy-done, bf16[256,256]{1,0:T(8,128)(2,1)S(1)} %copy-done.1, ...), custom_call_target="tpu_custom_call" | custom-call | flops 8000000000 | bytes 4000000 | tf_op jit(solution)/shard_map/segment_grads/pallas_call | solution.py:199
  13.4 34.1 %all-to-all-start = ((f32[128,2,128]{2,1,0:T(2,128)}), f32[128,2,128]{2,1,0:T(2,128)S(1)}, u32[]{:S(2)}, u32[]{:S(2)}) async-start(f32[128,2,128]{2,1,0:T(2,128)} %bitcast), calls=%async_computation | async-start | bytes 262144 | tf_op jit(solution)/shard_map/all_to_all | solution.py:208
  47.5 1.3 %collective-permute-start.2 = (bf16[256,256]{1,0:T(8,128)(2,1)S(1)}, bf16[256,256]{1,0:T(8,128)(2,1)S(1)}, u32[]{:S(2)}, u32[]{:S(2)}) collective-permute-start(bf16[256,256]{1,0:T(8,128)(2,1)S(1)} %get-tuple-element.12), channel_id=1, source_target_pairs={{8,0},{16,8},{24,16},{32,24},{40,32},{48,40},{56,48},{64,56},{72,6... | collective-permute-start | bytes 393224 | tf_op jit(solution)/shard_map/ppermute | solution.py:179
  48.8 1.3 %collective-permute-start.3 = (bf16[256,256]{1,0:T(8,128)(2,1)S(1)}, bf16[256,256]{1,0:T(8,128)(2,1)S(1)}, u32[]{:S(2)}, u32[]{:S(2)}) collective-permute-start(bf16[256,256]{1,0:T(8,128)(2,1)S(1)} %get-tuple-element.14), channel_id=1, source_target_pairs={{8,0},{16,8},{24,16},{32,24},{40,32},{48,40},{56,48},{64,56},{72,6... | collective-permute-start | bytes 393224 | tf_op jit(solution)/shard_map/ppermute | solution.py:179
  50.1 3.5 %collective-permute-done.2 = bf16[256,256]{1,0:T(8,128)(2,1)S(1)} collective-permute-done((bf16[256,256]{1,0:T(8,128)(2,1)S(1)}, bf16[256,256]{1,0:T(8,128)(2,1)S(1)}, u32[]{:S(2)}, u32[]{:S(2)}) %collective-permute-start.2) | collective-permute-done | bytes 131104 | tf_op jit(solution)/shard_map/ppermute | solution.py:179
  53.6 0.7 add_convert_fusion.1
  54.3 17.5 %all-to-all-done = f32[128,2,128]{2,1,0:T(2,128)S(1)} async-done(((f32[128,2,128]{2,1,0:T(2,128)}), f32[128,2,128]{2,1,0:T(2,128)S(1)}, u32[]{:S(2)}, u32[]{:S(2)}) %all-to-all-start) | async-done | bytes 131104 | tf_op jit(solution)/shard_map/all_to_all | solution.py:208
  71.8 0.1 reduce_sum.18
  71.9 0.6 broadcast_in_dim.3
  72.5 11.0 %all-to-all-start.1 = ((f32[8,2,128]{2,1,0:T(2,128)}), f32[8,2,128]{2,1,0:T(2,128)S(1)}, u32[]{:S(2)}, u32[]{:S(2)}) async-start(f32[8,2,128]{2,1,0:T(2,128)} %broadcast_in_dim.3), calls=%async_computation.1 | async-start | bytes 16384 | tf_op jit(solution)/shard_map/all_to_all | solution.py:211
  83.5 0.0 collective-permute-done.3
  83.5 0.7 add_convert_fusion
  84.2 3.9 %all-to-all-done.1 = f32[8,2,128]{2,1,0:T(2,128)S(1)} async-done(((f32[8,2,128]{2,1,0:T(2,128)}), f32[8,2,128]{2,1,0:T(2,128)S(1)}, u32[]{:S(2)}, u32[]{:S(2)}) %all-to-all-start.1) | async-done | bytes 8224 | tf_op jit(solution)/shard_map/all_to_all | solution.py:211
  88.2 0.6 reduce_sum.19
Async XLA Ops:
  0.6 8.6 %collective-permute-start = (bf16[256,256]{1,0:T(8,128)(2,1)}, bf16[256,256]{1,0:T(8,128)(2,1)S(1)}, u32[]{:S(2)}, u32[]{:S(2)}) collective-permute-start(bf16[256,256]{1,0:T(8,128)(2,1)} %key_ref.1), channel_id=1, source_target_pairs={{0,8},{8,16},{16,24},{24,32},{32,40},{40,48},{48,56},{56,64},{64,7... | collective-permute-start | bytes 393224 | tf_op jit(solution)/shard_map/ppermute | solution.py:179
  4.7 5.5 %collective-permute-start.1 = (bf16[256,256]{1,0:T(8,128)(2,1)}, bf16[256,256]{1,0:T(8,128)(2,1)S(1)}, u32[]{:S(2)}, u32[]{:S(2)}) collective-permute-start(bf16[256,256]{1,0:T(8,128)(2,1)} %value_ref.1), channel_id=1, source_target_pairs={{0,8},{8,16},{16,24},{24,32},{32,40},{40,48},{48,56},{56,64},{64,7... | collective-permute-start | bytes 393224 | tf_op jit(solution)/shard_map/ppermute | solution.py:179
  8.7 1.4 %copy-start = (bf16[256,256]{1,0:T(8,128)(2,1)S(1)}, bf16[256,256]{1,0:T(8,128)(2,1)}, u32[]{:S(2)}) copy-start(bf16[256,256]{1,0:T(8,128)(2,1)} %query_ref.1) | copy-start | bytes 393220
  8.7 1.4 %copy-start.1 = (bf16[256,256]{1,0:T(8,128)(2,1)S(1)}, bf16[256,256]{1,0:T(8,128)(2,1)}, u32[]{:S(2)}) copy-start(bf16[256,256]{1,0:T(8,128)(2,1)} %key_ref.1) | copy-start | bytes 393220
  8.8 1.4 %copy-start.2 = (bf16[256,256]{1,0:T(8,128)(2,1)S(1)}, bf16[256,256]{1,0:T(8,128)(2,1)}, u32[]{:S(2)}) copy-start(bf16[256,256]{1,0:T(8,128)(2,1)} %value_ref.1) | copy-start | bytes 393220
  8.8 1.4 %copy-start.3 = (bf16[256,256]{1,0:T(8,128)(2,1)S(1)}, bf16[256,256]{1,0:T(8,128)(2,1)}, u32[]{:S(2)}) copy-start(bf16[256,256]{1,0:T(8,128)(2,1)} %dout_ref.1) | copy-start | bytes 393220
  13.4 58.4 %all-to-all-start = ((f32[128,2,128]{2,1,0:T(2,128)}), f32[128,2,128]{2,1,0:T(2,128)S(1)}, u32[]{:S(2)}, u32[]{:S(2)}) async-start(f32[128,2,128]{2,1,0:T(2,128)} %bitcast), calls=%async_computation | async-start | bytes 262144 | tf_op jit(solution)/shard_map/all_to_all | solution.py:208
  47.5 6.1 %collective-permute-start.2 = (bf16[256,256]{1,0:T(8,128)(2,1)S(1)}, bf16[256,256]{1,0:T(8,128)(2,1)S(1)}, u32[]{:S(2)}, u32[]{:S(2)}) collective-permute-start(bf16[256,256]{1,0:T(8,128)(2,1)S(1)} %get-tuple-element.12), channel_id=1, source_target_pairs={{8,0},{16,8},{24,16},{32,24},{40,32},{48,40},{56,48},{64,56},{72,6... | collective-permute-start | bytes 393224 | tf_op jit(solution)/shard_map/ppermute | solution.py:179
  48.8 34.8 %collective-permute-start.3 = (bf16[256,256]{1,0:T(8,128)(2,1)S(1)}, bf16[256,256]{1,0:T(8,128)(2,1)S(1)}, u32[]{:S(2)}, u32[]{:S(2)}) collective-permute-start(bf16[256,256]{1,0:T(8,128)(2,1)S(1)} %get-tuple-element.14), channel_id=1, source_target_pairs={{8,0},{16,8},{24,16},{32,24},{40,32},{48,40},{56,48},{64,56},{72,6... | collective-permute-start | bytes 393224 | tf_op jit(solution)/shard_map/ppermute | solution.py:179
  72.5 15.7 %all-to-all-start.1 = ((f32[8,2,128]{2,1,0:T(2,128)}), f32[8,2,128]{2,1,0:T(2,128)S(1)}, u32[]{:S(2)}, u32[]{:S(2)}) async-start(f32[8,2,128]{2,1,0:T(2,128)} %broadcast_in_dim.3), calls=%async_computation.1 | async-start | bytes 16384 | tf_op jit(solution)/shard_map/all_to_all | solution.py:211

commit v2 on v1

--- a/solution.py
+++ b/solution.py
@@ -68,6 +68,7 @@
 def grads_kernel(
     first_head,
     is_first,
+    all_heads,
     query_ref,
     key_ref,
     value_ref,
@@ -76,10 +77,8 @@
     halo_value_ref,
     bias_ref,
     dquery_ref,
-    dkey_ref,
-    dvalue_ref,
-    back_key_ref,
-    back_value_ref,
+    own_ref,
+    back_ref,
     table_ref,
 ):
     rows, width = query_ref.shape
@@ -100,7 +99,7 @@
         parts.append(own_ref[max(start - REACH, 0) : stop, :])
         return jnp.concatenate(parts, axis=0)
 
-    dscore_sum = None
+    dscore_sum, held = None, []
     for pair in range(rows // PAIR):
         start = pair * PAIR
         halo_rows = max(REACH - start, 0)
@@ -128,20 +127,16 @@
         for h in range(1, heads):
             dquery = jnp.where(lane_head == h, stacked[h * PAIR : (h + 1) * PAIR], dquery)
         dquery_ref[start : start + PAIR, :] = dquery.astype(jnp.bfloat16)
-        if pair == 0:
-            back_key_ref[...] = dkey[:REACH].astype(jnp.bfloat16)
-            back_value_ref[...] = dvalue[:REACH].astype(jnp.bfloat16)
-            held_key = dkey[PAIR:REACH]
-            held_value = dvalue[PAIR:REACH]
-            dkey_ref[0:PAIR, :] = dkey[REACH:]
-            dvalue_ref[0:PAIR, :] = dvalue[REACH:]
-        else:
-            back_key_ref[PAIR:REACH, :] = (held_key + dkey[:PAIR]).astype(jnp.bfloat16)
-            back_value_ref[PAIR:REACH, :] = (held_value + dvalue[:PAIR]).astype(jnp.bfloat16)
-            dkey_ref[0:PAIR, :] += dkey[PAIR:REACH]
-            dvalue_ref[0:PAIR, :] += dvalue[PAIR:REACH]
-            dkey_ref[PAIR:, :] = dkey[REACH:]
-            dvalue_ref[PAIR:, :] = dvalue[REACH:]
+        for at, grad in ((0, dkey), (REACH, dvalue)):
+            own, back = own_ref.at[at : at + REACH, :], back_ref.at[at : at + REACH, :]
+            if pair == 0:
+                back[0:PAIR, :] = grad[:PAIR].astype(jnp.bfloat16)
+                held.append(grad[PAIR:REACH])
+                own[0:PAIR, :] = grad[REACH:]
+            else:
+                back[PAIR:, :] = (held.pop(0) + grad[:PAIR]).astype(jnp.bfloat16)
+                own[0:PAIR, :] += grad[PAIR:REACH]
+                own[PAIR:, :] = grad[REACH:]
 
     key_of = lax.broadcasted_iota(jnp.int32, (PAIR, PAIR), 0)
     query_of = lax.broadcasted_iota(jnp.int32, (PAIR, PAIR), 1)
@@ -155,15 +150,40 @@
         tops.append(jnp.sum(far + jnp.where(after, middle, 0.0), axis=0, keepdims=True))
     sums = diagonals(squares)
     last = lax.broadcasted_iota(jnp.int32, (1, PAIR), 1) == PAIR - 1
-    pad = [jnp.zeros((8 - heads, PAIR), jnp.float32)]
-    neg = jnp.concatenate(sums[0::2] + pad, axis=0)
-    pos = jnp.concatenate(
-        [s + jnp.where(last, jnp.sum(t, axis=1, keepdims=True), 0.0) for s, t in zip(sums[1::2], tops)] + pad, axis=0
+    pos = [s + jnp.where(last, jnp.sum(t, axis=1, keepdims=True), 0.0) for s, t in zip(sums[1::2], tops)]
+    table_ref[...] = by_owner(sums[0::2], pos, table_ref.shape[0], first_head(heads), all_heads)
+
+
+def by_owner(neg, pos, ranks, start, all_heads):
+    share = 2 * CLIP // ranks
+    half = ranks // 2
+    heads = len(neg)
+    mine = lax.broadcasted_iota(jnp.int32, (half, CLIP), 1) // share == lax.broadcasted_iota(jnp.int32, (half, CLIP), 0)
+    spread = jnp.concatenate(
+        [jnp.concatenate([jnp.where(mine, row, 0.0) for row in rows], axis=1) for rows in (neg, pos)], axis=0
     )
-    place = lax.broadcasted_iota(jnp.int32, (8, PAIR), 1) == lax.broadcasted_iota(jnp.int32, (8, PAIR), 0) + first_head(heads)
-    place = jnp.where(place & (lax.broadcasted_iota(jnp.int32, (8, PAIR), 0) < heads), 1.0, 0.0)
-    table_ref[0:CLIP, :] = dot(neg, place, TN, precision=HIGHEST)
-    table_ref[CLIP:, :] = dot(pos, place, TN, precision=HIGHEST)
+    source = lax.broadcasted_iota(jnp.int32, (heads * CLIP, PAIR), 0)
+    lane = lax.broadcasted_iota(jnp.int32, (heads * CLIP, PAIR), 1)
+    place = jnp.where(lane == source % share * all_heads + start + source // CLIP, 1.0, 0.0)
+    return dot(spread, place, NN, precision=HIGHEST)
+
+
+def add_kernel(own_ref, arrived_ref, dkey_ref, dvalue_ref):
+    rows = dkey_ref.shape[0]
+    for at, out_ref in ((0, dkey_ref), (rows, dvalue_ref)):
+        total = own_ref[at : at + rows, :] + arrived_ref[at : at + rows, :].astype(jnp.float32)
+        out_ref[...] = total.astype(jnp.bfloat16)
+
+
+def sum_kernel(terms_ref, copies_ref):
+    copies_ref[...] = jnp.broadcast_to(jnp.sum(terms_ref[...], axis=0, keepdims=True), copies_ref.shape)
+
+
+def table_kernel(copies_ref, out_ref):
+    row = jnp.sum(copies_ref[...], axis=0, keepdims=True)
+    share, heads = out_ref.shape
+    for r in range(share):
+        out_ref[r : r + 1, :] = row[:, r * heads : (r + 1) * heads]
 
 
 def first_head(heads):
@@ -195,21 +215,40 @@
         name="bias_tile",
     )(rel_bias)
     half = jax.ShapeDtypeStruct((rows, width), jnp.bfloat16)
-    full = jax.ShapeDtypeStruct((rows, width), jnp.float32)
-    query_grad, key_own, value_own, back_keys, back_values, table = pl.pallas_call(
-        partial(grads_kernel, first_head, is_first),
-        out_shape=(half, full, full, half, half, jax.ShapeDtypeStruct((table_rows, PAIR), jnp.float32)),
+    query_grad, own, back, table = pl.pallas_call(
+        partial(grads_kernel, first_head, is_first, all_heads),
+        out_shape=(
+            half,
+            jax.ShapeDtypeStruct((2 * rows, width), jnp.float32),
+            jax.ShapeDtypeStruct((2 * REACH, width), jnp.bfloat16),
+            jax.ShapeDtypeStruct((ranks, PAIR), jnp.float32),
+        ),
         cost_estimate=pl.CostEstimate(flops=8_000_000_000, bytes_accessed=4_000_000, transcendentals=0),
         compiler_params=pltpu.CompilerParams(vmem_limit_bytes=24 << 20),
         name="segment_grads",
     )(query_rows, key_rows, value_rows, out_grad, halo_keys, halo_values, bias)
-    key_grad = (key_own + passed_along(back_keys, -1)).astype(jnp.bfloat16)
-    value_grad = (value_own + passed_along(back_values, -1)).astype(jnp.bfloat16)
-    terms = lax.all_to_all(table.reshape(ranks, share, PAIR), "sp", 0, 0, tiled=True)
-    mine = jnp.sum(terms, axis=0)
+    key_grad, value_grad = pl.pallas_call(
+        add_kernel,
+        out_shape=(half, half),
+        cost_estimate=pl.CostEstimate(flops=1_000_000_000, bytes_accessed=1_000_000, transcendentals=0),
+        compiler_params=pltpu.CompilerParams(vmem_limit_bytes=4 << 20),
+        name="add_arrived",
+    )(own, passed_along(back, -1))
+    terms = lax.all_to_all(table.reshape(ranks, 1, PAIR), "sp", 0, 0, tiled=True)
     groups = lax.axis_size("tp")
-    copies = lax.all_to_all(jnp.broadcast_to(mine, (groups, share, PAIR)), "tp", 0, 0, tiled=True)
-    table_grad = jnp.sum(copies, axis=0)[:, :all_heads]
+    copies = pl.pallas_call(
+        sum_kernel,
+        out_shape=jax.ShapeDtypeStruct((groups, PAIR), jnp.float32),
+        compiler_params=pltpu.CompilerParams(vmem_limit_bytes=4 << 20),
+        name="sum_of_ranks",
+    )(terms.reshape(ranks, PAIR))
+    copies = lax.all_to_all(copies.reshape(groups, 1, PAIR), "tp", 0, 0, tiled=True)
+    table_grad = pl.pallas_call(
+        table_kernel,
+        out_shape=jax.ShapeDtypeStruct((share, all_heads), jnp.float32),
+        compiler_params=pltpu.CompilerParams(vmem_limit_bytes=4 << 20),
+        name="table_rows",
+    )(copies.reshape(groups, PAIR))
     return query_grad, key_grad, value_grad, table_grad
 
 

time: 89.1 us -> 84.7 us (0.951)
  starting transfers between devices: 55 us -> 50.4 us
  other arithmetic: 2.09 us -> 0 us
  Pallas kernels: 3.71 us -> 5.72 us
  waiting for transfers between devices: 25.8 us -> 26.7 us
    all_to_all x2, waiting for transfers between devices: 21.4 us -> 25.9 us  [the longest x1 22 us: shards(): lax.all_to_all(table.reshape(ranks, 1, PAIR), 'sp', 0, 0, tiled=True)]
    ppermute x4 -> x3, waiting for transfers between devices: 4.36 us -> 0.85 us  [passed_along(): lax.ppermute(block, 'sp', [(i - distance, i) for i in devices if i - dist...]
    all_to_all x2, starting transfers between devices: 45.1 us -> 41.8 us  [the longest x1 34.1 us: shards(): lax.all_to_all(table.reshape(ranks, 1, PAIR), 'sp', 0, 0, tiled=True)]
    pallas_call x1 -> x4, Pallas kernels: 3.23 us -> 5.25 us  [the longest x1 3.27 us: shards(): pl.pallas_call(partial(grads_kernel, first_head, is_first, all_heads), ou...]
    convert_element_type x2 -> x0, other arithmetic: 1.37 us -> none  [the longest x1 0.69 us: shards(): key_grad = (key_own + passed_along(back_keys, -1)).astype(jnp.bfloat16)]
    ppermute x4 -> x3, starting transfers between devices: 9.82 us -> 8.53 us  [passed_along(): lax.ppermute(block, 'sp', [(i - distance, i) for i in devices if i - dist...]
  transfers between devices with their start and end apart: 6 -> 5, of which waited for: 4 -> 3; matrix products, arithmetic and copies ran while one was open for 3% -> 1% of each run, Pallas kernels for 1% -> 2%
where the time goes in v2:
time: 84.7 us; the launch traced here: 84.4 us
  starting transfers between devices  50.4 us (60%)
  waiting for transfers between devices  26.7 us (32%)
  Pallas kernels  5.72 us (7%)
  local copies, waits for them, and re-layouts  0.88 us (1%)
    all_to_all x1, starting transfers between devices, shards(): lax.all_to_all(table.reshape(ranks, 1, PAIR), 'sp', 0, 0, tiled=True)  34.1 us
    all_to_all x1, waiting for transfers between devices, shards(): lax.all_to_all(table.reshape(ranks, 1, PAIR), 'sp', 0, 0, tiled=True)  22 us
    ppermute x3, starting transfers between devices, passed_along(): lax.ppermute(block, 'sp', [(i - distance, i) for i in devices if i - dist...  8.53 us
    all_to_all x1, starting transfers between devices, shards(): lax.all_to_all(copies.reshape(groups, 1, PAIR), 'tp', 0, 0, tiled=True)  7.75 us
    all_to_all x1, waiting for transfers between devices, shards(): lax.all_to_all(copies.reshape(groups, 1, PAIR), 'tp', 0, 0, tiled=True)  3.87 us
    pallas_call x1, Pallas kernels, shards(): pl.pallas_call(partial(grads_kernel, first_head, is_first, all_heads), ou...  3.27 us
  transfers between devices with their start and end apart: 5, of which 3 were waited for; matrix products, arithmetic and copies ran while one was open for 1% of the time, Pallas kernels for 2%

profile of v2, /device:TPU:1, one launch (start us, length us, event | category | flops | bytes accessed | tf_op | source)
XLA Modules:
  0.0 84.4 jit_solution(5268048063070659142)
XLA Ops:
  0.6 4.0 %collective-permute-start = (bf16[256,256]{1,0:T(8,128)(2,1)}, bf16[256,256]{1,0:T(8,128)(2,1)S(1)}, u32[]{:S(2)}, u32[]{:S(2)}) collective-permute-start(bf16[256,256]{1,0:T(8,128)(2,1)} %key_ref.1), channel_id=1, source_target_pairs={{0,8},{8,16},{16,24},{24,32},{32,40},{40,48},{48,56},{56,64},{64,7... | collective-permute-start | bytes 393224 | tf_op jit(solution)/shard_map/ppermute | solution.py:199
  4.7 3.2 %collective-permute-start.1 = (bf16[256,256]{1,0:T(8,128)(2,1)}, bf16[256,256]{1,0:T(8,128)(2,1)S(1)}, u32[]{:S(2)}, u32[]{:S(2)}) collective-permute-start(bf16[256,256]{1,0:T(8,128)(2,1)} %value_ref.1), channel_id=1, source_target_pairs={{0,8},{8,16},{16,24},{24,32},{32,40},{40,48},{48,56},{56,64},{64,7... | collective-permute-start | bytes 393224 | tf_op jit(solution)/shard_map/ppermute | solution.py:199
  7.9 0.9 %copy.10.table_ref = f32[256,32]{1,0:T(8,128)S(1)} copy(f32[256,32]{0,1:T(8,128)} %param.9) | data formatting | bytes 65536 | tf_op args[4]
  8.7 0.0 copy-start
  8.7 0.0 copy-start.1
  8.8 0.0 copy-start.2
  8.8 0.0 copy-start.3
  8.8 0.5 bias_tile.1.bias_ref
  9.3 0.0 collective-permute-done.halo_key_ref
  9.3 0.8 %collective-permute-done.1.halo_value_ref = bf16[256,256]{1,0:T(8,128)(2,1)S(1)} collective-permute-done((bf16[256,256]{1,0:T(8,128)(2,1)}, bf16[256,256]{1,0:T(8,128)(2,1)S(1)}, u32[]{:S(2)}, u32[]{:S(2)}) %collective-permute-start.1) | collective-permute-done | bytes 131104 | tf_op jit(solution)/shard_map/ppermute | solution.py:199
  10.1 0.0 copy-done
  10.1 0.0 copy-done.1
  10.1 0.0 copy-done.2
  10.1 0.0 copy-done.3
  10.1 3.3 %segment_grads.1 = (bf16[256,256]{1,0:T(8,128)(2,1)}, f32[512,256]{1,0:T(8,128)S(1)}, bf16[512,256]{1,0:T(8,128)(2,1)S(1)}, f32[128,128]{1,0:T(8,128)}) custom-call(bf16[256,256]{1,0:T(8,128)(2,1)S(1)} %copy-done, bf16[256,256]{1,0:T(8,128)(2,1)S(1)} %copy-done.1, bf16[256,256]{1,0:T(8,128)(2,1)S(1)} %copy-done.2, bf16[256,256]{1,0:T(8,128)(2,1)S(1)} %copy-done.3, ...), custom_call_target="tpu_custom_call" | custom-call | flops 8000000000 | bytes 4000000 | tf_op jit(solution)/shard_map/segment_grads/pallas_call | solution.py:218
  13.4 34.1 %all-to-all-start = ((f32[128,1,128]{2,1,0:T(1,128)}), f32[128,1,128]{2,1,0:T(1,128)S(1)}, u32[]{:S(2)}, u32[]{:S(2)}) async-start(f32[128,1,128]{2,1,0:T(1,128)} %bitcast.1), calls=%async_computation | async-start | bytes 131072 | tf_op jit(solution)/shard_map/all_to_all | solution.py:237
  47.5 1.3 %collective-permute-start.2 = (bf16[512,256]{1,0:T(8,128)(2,1)S(1)}, bf16[512,256]{1,0:T(8,128)(2,1)S(1)}, u32[]{:S(2)}, u32[]{:S(2)}) collective-permute-start(bf16[512,256]{1,0:T(8,128)(2,1)S(1)} %get-tuple-element.12), channel_id=1, source_target_pairs={{8,0},{16,8},{24,16},{32,24},{40,32},{48,40},{56,48},{64,56},{72,6... | collective-permute-start | bytes 786440 | tf_op jit(solution)/shard_map/ppermute | solution.py:199
  48.8 22.0 %all-to-all-done = f32[128,1,128]{2,1,0:T(1,128)S(1)} async-done(((f32[128,1,128]{2,1,0:T(1,128)}), f32[128,1,128]{2,1,0:T(1,128)S(1)}, u32[]{:S(2)}, u32[]{:S(2)}) %all-to-all-start) | async-done | bytes 65568 | tf_op jit(solution)/shard_map/all_to_all | solution.py:237
  70.8 0.6 sum_of_ranks.1
  71.4 7.8 %all-to-all-start.1 = ((f32[8,1,128]{2,1,0:T(1,128)}), f32[8,1,128]{2,1,0:T(1,128)S(1)}, u32[]{:S(2)}, u32[]{:S(2)}) async-start(f32[8,1,128]{2,1,0:T(1,128)} %bitcast.4), calls=%async_computation.1 | async-start | bytes 8192 | tf_op jit(solution)/shard_map/all_to_all | solution.py:245
  79.2 0.0 collective-permute-done.2.arrived_ref
  79.2 0.7 add_arrived.1
  79.9 3.9 %all-to-all-done.1 = f32[8,1,128]{2,1,0:T(1,128)S(1)} async-done(((f32[8,1,128]{2,1,0:T(1,128)}), f32[8,1,128]{2,1,0:T(1,128)S(1)}, u32[]{:S(2)}, u32[]{:S(2)}) %all-to-all-start.1) | async-done | bytes 4128 | tf_op jit(solution)/shard_map/all_to_all | solution.py:245
  83.8 0.6 table_rows.1
Async XLA Ops:
  0.6 8.6 %collective-permute-start = (bf16[256,256]{1,0:T(8,128)(2,1)}, bf16[256,256]{1,0:T(8,128)(2,1)S(1)}, u32[]{:S(2)}, u32[]{:S(2)}) collective-permute-start(bf16[256,256]{1,0:T(8,128)(2,1)} %key_ref.1), channel_id=1, source_target_pairs={{0,8},{8,16},{16,24},{24,32},{32,40},{40,48},{48,56},{56,64},{64,7... | collective-permute-start | bytes 393224 | tf_op jit(solution)/shard_map/ppermute | solution.py:199
  4.7 5.5 %collective-permute-start.1 = (bf16[256,256]{1,0:T(8,128)(2,1)}, bf16[256,256]{1,0:T(8,128)(2,1)S(1)}, u32[]{:S(2)}, u32[]{:S(2)}) collective-permute-start(bf16[256,256]{1,0:T(8,128)(2,1)} %value_ref.1), channel_id=1, source_target_pairs={{0,8},{8,16},{16,24},{24,32},{32,40},{40,48},{48,56},{56,64},{64,7... | collective-permute-start | bytes 393224 | tf_op jit(solution)/shard_map/ppermute | solution.py:199
  8.7 1.4 %copy-start = (bf16[256,256]{1,0:T(8,128)(2,1)S(1)}, bf16[256,256]{1,0:T(8,128)(2,1)}, u32[]{:S(2)}) copy-start(bf16[256,256]{1,0:T(8,128)(2,1)} %query_ref.1) | copy-start | bytes 393220
  8.7 1.4 %copy-start.1 = (bf16[256,256]{1,0:T(8,128)(2,1)S(1)}, bf16[256,256]{1,0:T(8,128)(2,1)}, u32[]{:S(2)}) copy-start(bf16[256,256]{1,0:T(8,128)(2,1)} %key_ref.1) | copy-start | bytes 393220
  8.8 1.4 %copy-start.2 = (bf16[256,256]{1,0:T(8,128)(2,1)S(1)}, bf16[256,256]{1,0:T(8,128)(2,1)}, u32[]{:S(2)}) copy-start(bf16[256,256]{1,0:T(8,128)(2,1)} %value_ref.1) | copy-start | bytes 393220
  8.8 1.4 %copy-start.3 = (bf16[256,256]{1,0:T(8,128)(2,1)S(1)}, bf16[256,256]{1,0:T(8,128)(2,1)}, u32[]{:S(2)}) copy-start(bf16[256,256]{1,0:T(8,128)(2,1)} %dout_ref.1) | copy-start | bytes 393220
  13.4 57.4 %all-to-all-start = ((f32[128,1,128]{2,1,0:T(1,128)}), f32[128,1,128]{2,1,0:T(1,128)S(1)}, u32[]{:S(2)}, u32[]{:S(2)}) async-start(f32[128,1,128]{2,1,0:T(1,128)} %bitcast.1), calls=%async_computation | async-start | bytes 131072 | tf_op jit(solution)/shard_map/all_to_all | solution.py:237
  47.5 31.7 %collective-permute-start.2 = (bf16[512,256]{1,0:T(8,128)(2,1)S(1)}, bf16[512,256]{1,0:T(8,128)(2,1)S(1)}, u32[]{:S(2)}, u32[]{:S(2)}) collective-permute-start(bf16[512,256]{1,0:T(8,128)(2,1)S(1)} %get-tuple-element.12), channel_id=1, source_target_pairs={{8,0},{16,8},{24,16},{32,24},{40,32},{48,40},{56,48},{64,56},{72,6... | collective-permute-start | bytes 786440 | tf_op jit(solution)/shard_map/ppermute | solution.py:199
  71.4 12.4 %all-to-all-start.1 = ((f32[8,1,128]{2,1,0:T(1,128)}), f32[8,1,128]{2,1,0:T(1,128)S(1)}, u32[]{:S(2)}, u32[]{:S(2)}) async-start(f32[8,1,128]{2,1,0:T(1,128)} %bitcast.4), calls=%async_computation.1 | async-start | bytes 8192 | tf_op jit(solution)/shard_map/all_to_all | solution.py:245

commit v3 on v1

v3 whole, which is shorter than its diff:
```python
from functools import partial

import jax
import jax.numpy as jnp
from jax import lax
from jax.experimental import pallas as pl
from jax.experimental.pallas import tpu as pltpu
from jax.sharding import Mesh
from jax.sharding import PartitionSpec as P

HEAD_DIM = 64
SEG = 64
LEFT = 4
CLIP = 128
NEG_FILL = -1e30
SP = ("z", "y")
PLANE = ("y", "tp")
HIGHEST = lax.Precision.HIGHEST

REACH = LEFT * SEG
PAIR = 2 * SEG
WIN = REACH + PAIR

NT = (((1,), (1,)), ((), ()))
TN = (((0,), (0,)), ((), ()))
NN = (((1,), (0,)), ((), ()))


def dot(a, b, dims, **kw):
    return lax.dot_general(a, b, dims, preferred_element_type=jnp.float32, **kw)


def bias_kernel(first_head, table_ref, bias_ref):
    heads = bias_ref.shape[1] // PAIR
    wide = table_ref.shape[1]
    start = first_head(heads)
    pick = lax.broadcasted_iota(jnp.int32, (8, wide), 1) == lax.broadcasted_iota(jnp.int32, (8, wide), 0) + start
    rows = dot(jnp.where(pick, 1.0, 0.0), table_ref[...], NT, precision=HIGHEST)
    key_of = lax.broadcasted_iota(jnp.int32, (PAIR, PAIR), 0)
    query_of = lax.broadcasted_iota(jnp.int32, (PAIR, PAIR), 1)
    early = query_of < SEG
    low = key_of < SEG
    after = query_of >= key_of
    for head in range(heads):
        lanes = slice(head * PAIR, (head + 1) * PAIR)
        neg = jnp.broadcast_to(rows[head : head + 1, :CLIP], (PAIR, PAIR))
        pos = jnp.broadcast_to(rows[head : head + 1, CLIP:], (PAIR, PAIR))
        neg = pltpu.roll(neg, 0, 1, stride=1, stride_axis=0)
        pos = pltpu.roll(pos, 0, 1, stride=1, stride_axis=0)
        top = rows[head : head + 1, 2 * CLIP - 1 :]
        bias_ref[0:PAIR, lanes] = jnp.where(low & ~early, NEG_FILL, jnp.broadcast_to(top, (PAIR, PAIR)))
        bias_ref[PAIR : 2 * PAIR, lanes] = jnp.where(after, top, pos)
        bias_ref[2 * PAIR : 3 * PAIR, lanes] = jnp.where(early & ~low, NEG_FILL, jnp.where(after, pos, neg))


def diagonals(squares):
    rows = PAIR
    while rows > 8:
        half = rows // 2
        squares = [s[:half] + pltpu.roll(s[half:], PAIR - half, 1) for s in squares]
        rows = half
    row_of = lax.broadcasted_iota(jnp.int32, (8, PAIR), 0)
    sums = []
    for s in squares:
        for bit in (4, 2, 1):
            s = jnp.where((row_of & bit) != 0, pltpu.roll(s, PAIR - bit, 1), s)
        sums.append(jnp.sum(s, axis=0, keepdims=True))
    return sums


def by_head(block, width):
    lane_head = lax.broadcasted_iota(jnp.int32, block.shape, 1) // HEAD_DIM
    zero = jnp.zeros_like(block)
    return jnp.concatenate([jnp.where(lane_head == h, block, zero) for h in range(width // HEAD_DIM)], axis=0)


def window(halo_ref, own_ref, pair):
    start = pair * PAIR
    parts = [halo_ref[start:REACH, :]] if start < REACH else []
    parts.append(own_ref[max(start - REACH, 0) : start + PAIR, :])
    return jnp.concatenate(parts, axis=0)


def probs_kernel(is_first, query_ref, key_ref, halo_ref, bias_ref, probs_ref, half_ref):
    rows, width = query_ref.shape
    halo_fill = jnp.where(is_first(), NEG_FILL, 0.0)
    for pair in range(rows // PAIR):
        start = pair * PAIR
        halo_rows = max(REACH - start, 0)
        query = by_head(query_ref[start : start + PAIR, :], width)
        scores = dot(window(halo_ref, key_ref, pair), query, NT) * HEAD_DIM**-0.5 + bias_ref[...]
        if halo_rows:
            scores = jnp.concatenate([scores[:halo_rows] + halo_fill, scores[halo_rows:]], axis=0)
        peak = jnp.max(scores, axis=0, keepdims=True)
        weights = jnp.exp(scores - peak)
        total = jnp.sum(weights, axis=0, keepdims=True)
        probs = weights * (1.0 / total)
        probs_ref[pair * WIN : (pair + 1) * WIN, :] = probs
        half_ref[pair * WIN : (pair + 1) * WIN, :] = probs.astype(jnp.bfloat16)


def dscores_kernel(value_ref, dout_ref, halo_ref, probs_ref, dscores_ref, table_ref):
    rows, width = value_ref.shape
    heads = width // HEAD_DIM
    dscore_sum = None
    for pair in range(rows // PAIR):
        start = pair * PAIR
        dout = by_head(dout_ref[start : start + PAIR, :], width)
        dprobs = dot(window(halo_ref, value_ref, pair), dout, NT)
        probs = probs_ref[pair * WIN : (pair + 1) * WIN, :]
        inner = jnp.sum(probs * dprobs, axis=0, keepdims=True)
        dscores = probs * (dprobs - inner)
        dscore_sum = dscores if dscore_sum is None else dscore_sum + dscores
        dscores_ref[pair * WIN : (pair + 1) * WIN, :] = dscores.astype(jnp.bfloat16)
    key_of = lax.broadcasted_iota(jnp.int32, (PAIR, PAIR), 0)
    query_of = lax.broadcasted_iota(jnp.int32, (PAIR, PAIR), 1)
    after = query_of >= key_of
    squares, tops = [], []
    for h in range(heads):
        lanes = slice(h * PAIR, (h + 1) * PAIR)
        far, middle, near = (dscore_sum[b * PAIR : (b + 1) * PAIR, lanes] for b in range(3))
        squares.append(jnp.where(after, 0.0, near))
        squares.append(jnp.where(after, near, middle))
        tops.append(jnp.sum(far + jnp.where(after, middle, 0.0), axis=0, keepdims=True))
    sums = diagonals(squares)
    last = lax.broadcasted_iota(jnp.int32, (1, PAIR), 1) == PAIR - 1
    pos = [s + jnp.where(last, jnp.sum(t, axis=1, keepdims=True), 0.0) for s, t in zip(sums[1::2], tops)]
    by_rank = by_owner(sums[0::2], pos)
    ranks = lax.axis_size("y")
    share = by_rank.shape[0] // ranks
    copies = table_ref.shape[0] // by_rank.shape[0]
    for y in range(ranks):
        block = jnp.concatenate([by_rank[y * share : (y + 1) * share, :]] * copies, axis=0)
        table_ref[y * share * copies : (y + 1) * share * copies, :] = block


def by_owner(neg, pos):
    heads = len(neg)
    period = 2 * CLIP // lax.axis_size("z")
    rows = lax.broadcasted_iota(jnp.int32, (period, CLIP), 0)
    mine = lax.broadcasted_iota(jnp.int32, (period, CLIP), 1) % period == rows
    spread = jnp.concatenate([jnp.where(mine, row, 0.0) for row in neg + pos], axis=1)
    source = lax.broadcasted_iota(jnp.int32, (2 * heads * CLIP, PAIR), 0)
    lane = lax.broadcasted_iota(jnp.int32, (2 * heads * CLIP, PAIR), 1)
    head = source // CLIP % heads
    index = source % CLIP + source // (heads * CLIP) * CLIP
    place = jnp.where(lane == index // period * heads + head, 1.0, 0.0)
    return dot(spread, place, NN, precision=HIGHEST)


def heads_kernel(heads, all_heads, terms_ref, out_ref):
    ranks, groups = lax.axis_size("z"), lax.axis_size("tp")
    share = 2 * CLIP // lax.axis_size(SP)
    each = groups * share
    total = terms_ref[0:each, :]
    for y in range(1, lax.axis_size("y")):
        total = total + terms_ref[y * each : (y + 1) * each, :]
    source = lax.broadcasted_iota(jnp.int32, (each, PAIR), 0)
    lane = lax.broadcasted_iota(jnp.int32, (each, PAIR), 1)
    wanted = (lane // all_heads == source % share) & (lane % all_heads // heads == source // share)
    spread = dot(total, jnp.where(wanted, 1.0, 0.0), TN, precision=HIGHEST)
    source = lax.broadcasted_iota(jnp.int32, (PAIR, PAIR), 0)
    lane = lax.broadcasted_iota(jnp.int32, (PAIR, PAIR), 1)
    spread = jnp.where(source % heads == lane % heads, spread, 0.0)
    rank = (lax.broadcasted_iota(jnp.int32, (ranks, PAIR), 0) + ranks // 2) % ranks
    pick = lax.broadcasted_iota(jnp.int32, (ranks, PAIR), 1) // heads == rank
    out_ref[...] = dot(jnp.where(pick, 1.0, 0.0), spread, NN, precision=HIGHEST)


def grads_kernel(
    query_ref, key_ref, dout_ref, halo_ref, probs_ref, dscores_ref, dquery_ref, own_ref, back_ref
):
    rows, width = query_ref.shape
    heads = width // HEAD_DIM
    scale = HEAD_DIM**-0.5
    lane_head = lax.broadcasted_iota(jnp.int32, (PAIR, width), 1) // HEAD_DIM
    held = []
    for pair in range(rows // PAIR):
        start = pair * PAIR
        query = by_head(query_ref[start : start + PAIR, :], width)
        dout = by_head(dout_ref[start : start + PAIR, :], width)
        prob_half = probs_ref[pair * WIN : (pair + 1) * WIN, :]
        dscore_half = dscores_ref[pair * WIN : (pair + 1) * WIN, :]
        dvalue = dot(prob_half, dout, NN)
        dkey = dot(dscore_half, query, NN) * scale
        stacked = dot(dscore_half, window(halo_ref, key_ref, pair), TN) * scale
        dquery = stacked[:PAIR]
        for h in range(1, heads):
            dquery = jnp.where(lane_head == h, stacked[h * PAIR : (h + 1) * PAIR], dquery)
        dquery_ref[start : start + PAIR, :] = dquery.astype(jnp.bfloat16)
        for at, grad in ((0, dkey), (REACH, dvalue)):
            own, back = own_ref.at[at : at + REACH, :], back_ref.at[at : at + REACH, :]
            if pair == 0:
                back[0:PAIR, :] = grad[:PAIR].astype(jnp.bfloat16)
                held.append(grad[PAIR:REACH])
                own[0:PAIR, :] = grad[REACH:]
            else:
                back[PAIR:, :] = (held.pop(0) + grad[:PAIR]).astype(jnp.bfloat16)
                own[0:PAIR, :] += grad[PAIR:REACH]
                own[PAIR:, :] = grad[REACH:]


def last_kernel(own_ref, arrived_ref, terms_ref, dkey_ref, dvalue_ref, table_ref):
    rows = dkey_ref.shape[0]
    for at, out_ref in ((0, dkey_ref), (rows, dvalue_ref)):
        total = own_ref[at : at + rows, :] + arrived_ref[at : at + rows, :].astype(jnp.float32)
        out_ref[...] = total.astype(jnp.bfloat16)
    row = jnp.sum(terms_ref[...], axis=0, keepdims=True)
    share, heads = table_ref.shape
    for r in range(share):
        table_ref[r : r + 1, :] = row[:, r * heads : (r + 1) * heads]


def first_head(heads):
    return lax.axis_index("tp") * heads


def is_first():
    return lax.axis_index(SP) == 0


def passed_along(block, distance):
    devices = range(lax.axis_size(SP))
    return lax.ppermute(block, SP, [(i - distance, i) for i in devices if i - distance in devices])


def kernel(body, outs, flops):
    return pl.pallas_call(
        body,
        out_shape=outs,
        cost_estimate=pl.CostEstimate(flops=flops, bytes_accessed=2_000_000, transcendentals=0),
        compiler_params=pltpu.CompilerParams(vmem_limit_bytes=16 << 20),
    )


def shards(query_rows, key_rows, value_rows, out_grad, rel_bias):
    rows, width = query_rows.shape
    heads = width // HEAD_DIM
    all_heads = rel_bias.shape[1]
    ranks, groups = lax.axis_size("z"), lax.axis_size(PLANE)
    share = 2 * CLIP // lax.axis_size(SP)
    pairs = rows // PAIR
    struct = jax.ShapeDtypeStruct
    half = struct((rows, width), jnp.bfloat16)
    wide = struct((pairs * WIN, heads * PAIR), jnp.float32)
    wide_half = struct(wide.shape, jnp.bfloat16)

    halo_keys = passed_along(key_rows, 1)
    halo_values = passed_along(value_rows, 1)
    bias_shape = struct((WIN, heads * PAIR), jnp.float32)
    bias = kernel(partial(bias_kernel, first_head), bias_shape, 2_000_000_000)(rel_bias)
    probs, prob_half = kernel(partial(probs_kernel, is_first), (wide, wide_half), 4_000_000_000)(
        query_rows, key_rows, halo_keys, bias
    )
    outs = (wide_half, struct((groups * share, PAIR), jnp.float32))
    dscores, table = kernel(dscores_kernel, outs, 4_000_000_000)(value_rows, out_grad, halo_values, probs)
    terms = lax.all_to_all(table.reshape(groups, share, PAIR), PLANE, 0, 0, tiled=True)
    outs = (half, struct((2 * rows, width), jnp.float32), struct((2 * REACH, width), jnp.bfloat16))
    query_grad, own, back = kernel(grads_kernel, outs, 4_000_000_000)(
        query_rows, key_rows, out_grad, halo_keys, prob_half, dscores
    )
    arrived = passed_along(back, -1)
    table = kernel(
        partial(heads_kernel, heads, all_heads), struct((ranks, PAIR), jnp.float32), 500_000_000
    )(terms.reshape(groups * share, PAIR))
    order = [[(i + ranks // 2) % ranks for i in range(ranks)]]
    terms = lax.all_to_all(table.reshape(ranks, 1, PAIR), "z", 0, 0, axis_index_groups=order, tiled=True)
    outs = (half, half, struct((share, all_heads), jnp.float32))
    key_grad, value_grad, table_grad = kernel(last_kernel, outs, 500_000_000)(own, arrived, terms.reshape(ranks, PAIR))
    return query_grad, key_grad, value_grad, table_grad


def solution(mesh):
    finer = Mesh(mesh.devices.reshape(-1, 4, mesh.shape["tp"]), ("z", "y", "tp"))
    return jax.shard_map(
        shards,
        mesh=finer,
        in_specs=(P(SP, "tp"), P(SP, "tp"), P(SP, "tp"), P(SP, "tp"), P()),
        out_specs=(P(SP, "tp"), P(SP, "tp"), P(SP, "tp"), P(SP, None)),
        check_vma=False,
    )
```

time: 89.1 us -> 72.8 us (0.82)
  blocking collectives: 0 us -> 55.4 us
  starting transfers between devices: 55 us -> 8.51 us
  waiting for transfers between devices: 25.8 us -> 0.86 us
  Pallas kernels: 3.71 us -> 6.07 us
  other arithmetic: 2.09 us -> 0 us
    all_to_all x0 -> x2, blocking collectives: none -> 55.4 us  [the longest x1 31.8 us: shards(): lax.all_to_all(table.reshape(ranks, 1, PAIR), 'z', 0, 0, axis_index_group...]
    all_to_all x2 -> x0, starting transfers between devices: 45.1 us -> none  [the longest x1 34.1 us: shards(): lax.all_to_all(table.reshape(ranks, share, PAIR), 'sp', 0, 0, tiled=True)]
    all_to_all x2 -> x0, waiting for transfers between devices: 21.4 us -> none  [the longest x1 17.5 us: shards(): lax.all_to_all(table.reshape(ranks, share, PAIR), 'sp', 0, 0, tiled=True)]
    ppermute x4 -> x3, waiting for transfers between devices: 4.36 us -> 0.86 us  [passed_along(): lax.ppermute(block, SP, [(i - distance, i) for i in devices if i - distan...]
    pallas_call x2 -> x6, Pallas kernels: 3.71 us -> 6.07 us  [the longest x1 1.87 us: shards(): kernel(dscores_kernel, outs, 4000000000)]
    convert_element_type x2 -> x0, other arithmetic: 1.37 us -> none  [the longest x1 0.69 us: shards(): key_grad = (key_own + passed_along(back_keys, -1)).astype(jnp.bfloat16)]
    ppermute x4 -> x3, starting transfers between devices: 9.82 us -> 8.51 us  [passed_along(): lax.ppermute(block, SP, [(i - distance, i) for i in devices if i - distan...]
  transfers between devices with their start and end apart: 6 -> 3, of which waited for: 4 -> 1; matrix products, arithmetic and copies ran while one was open for 3% -> 1% of each run, Pallas kernels for 1% -> 3%
where the time goes in v3:
time: 72.8 us; the launch traced here: 72.5 us
  blocking collectives  55.4 us (76%)
  starting transfers between devices  8.51 us (12%)
  Pallas kernels  6.07 us (8%)
  local copies, waits for them, and re-layouts  0.88 us (1%)
  waiting for transfers between devices  0.86 us (1%)
  between operations  0.73 us (1%)
    all_to_all x1, blocking collectives, shards(): lax.all_to_all(table.reshape(ranks, 1, PAIR), 'z', 0, 0, axis_index_group...  31.8 us
    all_to_all x1, blocking collectives, shards(): lax.all_to_all(table.reshape(groups, share, PAIR), PLANE, 0, 0, tiled=True)  23.7 us
    ppermute x3, starting transfers between devices, passed_along(): lax.ppermute(block, SP, [(i - distance, i) for i in devices if i - distan...  8.51 us
    pallas_call x1, Pallas kernels, shards(): kernel(dscores_kernel, outs, 4000000000)  1.87 us
    pallas_call x1, Pallas kernels, shards(): kernel(grads_kernel, outs, 4000000000)  1.53 us
  transfers between devices with their start and end apart: 3, of which 1 were waited for; matrix products, arithmetic and copies ran while one was open for 1% of the time, Pallas kernels for 3%

profile of v3, /device:TPU:1, one launch (start us, length us, event | category | flops | bytes accessed | tf_op | source)
XLA Modules:
  0.0 72.5 jit_solution(5743687925983941326)
XLA Ops:
  0.6 4.0 %collective-permute-start.1 = (bf16[256,256]{1,0:T(8,128)(2,1)}, bf16[256,256]{1,0:T(8,128)(2,1)S(1)}, u32[]{:S(2)}, u32[]{:S(2)}) collective-permute-start(bf16[256,256]{1,0:T(8,128)(2,1)} %value_ref.1), channel_id=1, source_target_pairs={{0,8},{8,16},{16,24},{24,32},{32,40},{40,48},{48,56},{56,64},{64,7... | collective-permute-start | bytes 393224 | tf_op jit(solution)/shard_map/ppermute | solution.py:224
  4.7 3.2 %collective-permute-start = (bf16[256,256]{1,0:T(8,128)(2,1)}, bf16[256,256]{1,0:T(8,128)(2,1)S(1)}, u32[]{:S(2)}, u32[]{:S(2)}) collective-permute-start(bf16[256,256]{1,0:T(8,128)(2,1)} %key_ref.3), channel_id=1, source_target_pairs={{0,8},{8,16},{16,24},{24,32},{32,40},{40,48},{48,56},{56,64},{64,7... | collective-permute-start | bytes 393224 | tf_op jit(solution)/shard_map/ppermute | solution.py:224
  7.9 0.9 %copy.10.table_ref = f32[256,32]{1,0:T(8,128)S(1)} copy(f32[256,32]{0,1:T(8,128)} %param.9) | data formatting | bytes 65536 | tf_op args[4]
  8.7 0.0 copy-start.1
  8.7 0.0 copy-start.2
  8.8 0.5 shard_map.84.bias_ref
  9.2 0.0 copy-start
  9.3 0.0 copy-start.3
  9.3 0.9 %collective-permute-done.halo_ref = bf16[256,256]{1,0:T(8,128)(2,1)S(1)} collective-permute-done((bf16[256,256]{1,0:T(8,128)(2,1)}, bf16[256,256]{1,0:T(8,128)(2,1)S(1)}, u32[]{:S(2)}, u32[]{:S(2)}) %collective-permute-start) | collective-permute-done | bytes 131104 | tf_op jit(solution)/shard_map/ppermute | solution.py:224
  10.1 0.0 copy-done.1
  10.1 0.0 copy-done.2
  10.1 0.9 %shard_map.85 = (f32[768,512]{1,0:T(8,128)S(1)}, bf16[768,512]{1,0:T(8,128)(2,1)S(1)}) custom-call(bf16[256,256]{1,0:T(8,128)(2,1)S(1)} %copy-done.1, bf16[256,256]{1,0:T(8,128)(2,1)S(1)} %copy-done.2, bf16[256,256]{1,0:T(8,128)(2,1)S(1)} %collective-permute-done.halo_ref, f32[384,512]{1,0:T(8,128)S(1)} %shard_map.84.bias_ref), custom_call_target="tpu_custom_call" | custom-call | flops 4000000000 | bytes 2000000 | tf_op jit(solution)/shard_map/pallas_call | solution.py:252
  11.1 0.0 collective-permute-done.1.halo_ref
  11.1 0.0 copy-done
  11.1 0.0 copy-done.3
  11.1 1.9 %shard_map.86 = (bf16[768,512]{1,0:T(8,128)(2,1)S(1)}, f32[64,128]{1,0:T(8,128)S(1)}) custom-call(bf16[256,256]{1,0:T(8,128)(2,1)S(1)} %copy-done, bf16[256,256]{1,0:T(8,128)(2,1)S(1)} %copy-done.3, bf16[256,256]{1,0:T(8,128)(2,1)S(1)} %collective-permute-done.1.halo_ref, f32[768,512]{1,0:T(8,128)S(1)} %get-tuple-element.15.probs_ref), custom_call_target="tpu_custom_call" | custom-call | flops 4000000000 | bytes 2000000 | tf_op jit(solution)/shard_map/pallas_call | solution.py:256
  13.0 1.5 %shard_map.87 = (bf16[256,256]{1,0:T(8,128)(2,1)}, f32[512,256]{1,0:T(8,128)S(1)}, bf16[512,256]{1,0:T(8,128)(2,1)S(1)}) custom-call(bf16[256,256]{1,0:T(8,128)(2,1)S(1)} %copy-done.1, bf16[256,256]{1,0:T(8,128)(2,1)S(1)} %copy-done.2, bf16[256,256]{1,0:T(8,128)(2,1)S(1)} %copy-done.3, bf16[256,256]{1,0:T(8,128)(2,1)S(1)} %collective-permute-done.halo_ref, ...), custom_call_target="tpu_custom_call" | custom-call | flops 4000000000 | bytes 2000000 | tf_op jit(solution)/shard_map/pallas_call | solution.py:259
  14.5 1.3 %collective-permute-start.2 = (bf16[512,256]{1,0:T(8,128)(2,1)S(1)}, bf16[512,256]{1,0:T(8,128)(2,1)S(1)}, u32[]{:S(2)}, u32[]{:S(2)}) collective-permute-start(bf16[512,256]{1,0:T(8,128)(2,1)S(1)} %get-tuple-element.19), channel_id=1, source_target_pairs={{8,0},{16,8},{24,16},{32,24},{40,32},{48,40},{56,48},{64,56},{72,6... | collective-permute-start | bytes 786440 | tf_op jit(solution)/shard_map/ppermute | solution.py:224
  15.8 23.7 %all_to_all.10 = f32[32,2,128]{2,1,0:T(2,128)S(1)} all-to-all(f32[32,2,128]{2,1,0:T(2,128)S(1)} %bitcast.6), channel_id=1, replica_groups=mesh['z'=32,'y'=4,'tp'=8] {'y','tp'}, dimensions={0} | all-to-all | bytes 65536 | tf_op jit(solution)/shard_map/all_to_all | solution.py:257
  39.5 0.5 shard_map.88
  40.0 31.8 %all_to_all.11 = f32[32,1,128]{2,1,0:T(1,128)S(1)} all-to-all(f32[32,1,128]{2,1,0:T(1,128)S(1)} %bitcast.9), channel_id=1, replica_groups={{512,544,576,608,640,672,704,736,768,800,832,864,896,928,960,992,0,32,6..., dimensions={0} | all-to-all | bytes 32768 | tf_op jit(solution)/shard_map/all_to_all | solution.py:267
  71.7 0.0 collective-permute-done.2.arrived_ref
  71.7 0.8 %shard_map.89 = (bf16[256,256]{1,0:T(8,128)(2,1)}, bf16[256,256]{1,0:T(8,128)(2,1)}, f32[2,32]{1,0:T(2,128)}) custom-call(f32[512,256]{1,0:T(8,128)S(1)} %get-tuple-element.18.own_ref, bf16[512,256]{1,0:T(8,128)(2,1)S(1)} %collective-permute-done.2.arrived_ref, f32[32,128]{1,0:T(8,128)S(1)} %bitcast.8), custom_call_target="tpu_custom_call" | custom-call | flops 500000000 | bytes 2000000 | tf_op jit(solution)/shard_map/pallas_call | solution.py:269
Async XLA Ops:
  0.6 10.4 %collective-permute-start.1 = (bf16[256,256]{1,0:T(8,128)(2,1)}, bf16[256,256]{1,0:T(8,128)(2,1)S(1)}, u32[]{:S(2)}, u32[]{:S(2)}) collective-permute-start(bf16[256,256]{1,0:T(8,128)(2,1)} %value_ref.1), channel_id=1, source_target_pairs={{0,8},{8,16},{16,24},{24,32},{32,40},{40,48},{48,56},{56,64},{64,7... | collective-permute-start | bytes 393224 | tf_op jit(solution)/shard_map/ppermute | solution.py:224
  4.7 5.5 %collective-permute-start = (bf16[256,256]{1,0:T(8,128)(2,1)}, bf16[256,256]{1,0:T(8,128)(2,1)S(1)}, u32[]{:S(2)}, u32[]{:S(2)}) collective-permute-start(bf16[256,256]{1,0:T(8,128)(2,1)} %key_ref.3), channel_id=1, source_target_pairs={{0,8},{8,16},{16,24},{24,32},{32,40},{40,48},{48,56},{56,64},{64,7... | collective-permute-start | bytes 393224 | tf_op jit(solution)/shard_map/ppermute | solution.py:224
  8.7 1.4 %copy-start.1 = (bf16[256,256]{1,0:T(8,128)(2,1)S(1)}, bf16[256,256]{1,0:T(8,128)(2,1)}, u32[]{:S(2)}) copy-start(bf16[256,256]{1,0:T(8,128)(2,1)} %query_ref.3) | copy-start | bytes 393220
  8.7 1.4 %copy-start.2 = (bf16[256,256]{1,0:T(8,128)(2,1)S(1)}, bf16[256,256]{1,0:T(8,128)(2,1)}, u32[]{:S(2)}) copy-start(bf16[256,256]{1,0:T(8,128)(2,1)} %key_ref.3) | copy-start | bytes 393220
  9.2 1.9 %copy-start = (bf16[256,256]{1,0:T(8,128)(2,1)S(1)}, bf16[256,256]{1,0:T(8,128)(2,1)}, u32[]{:S(2)}) copy-start(bf16[256,256]{1,0:T(8,128)(2,1)} %value_ref.1) | copy-start | bytes 393220
  9.3 1.8 %copy-start.3 = (bf16[256,256]{1,0:T(8,128)(2,1)S(1)}, bf16[256,256]{1,0:T(8,128)(2,1)}, u32[]{:S(2)}) copy-start(bf16[256,256]{1,0:T(8,128)(2,1)} %dout_ref.3) | copy-start | bytes 393220
  14.5 57.2 %collective-permute-start.2 = (bf16[512,256]{1,0:T(8,128)(2,1)S(1)}, bf16[512,256]{1,0:T(8,128)(2,1)S(1)}, u32[]{:S(2)}, u32[]{:S(2)}) collective-permute-start(bf16[512,256]{1,0:T(8,128)(2,1)S(1)} %get-tuple-element.19), channel_id=1, source_target_pairs={{8,0},{16,8},{24,16},{32,24},{40,32},{48,40},{56,48},{64,56},{72,6... | collective-permute-start | bytes 786440 | tf_op jit(solution)/shard_map/ppermute | solution.py:224

commit v4 on v3

--- a/solution.py
+++ b/solution.py
@@ -99,33 +99,47 @@
         half_ref[pair * WIN : (pair + 1) * WIN, :] = probs.astype(jnp.bfloat16)
 
 
+def thirds(block):
+    high = block.astype(jnp.bfloat16)
+    rest = block - high.astype(jnp.float32)
+    middle = rest.astype(jnp.bfloat16)
+    return high, middle, (rest - middle.astype(jnp.float32)).astype(jnp.bfloat16)
+
+
 def dscores_kernel(value_ref, dout_ref, halo_ref, probs_ref, dscores_ref, table_ref):
     rows, width = value_ref.shape
     heads = width // HEAD_DIM
-    dscore_sum = None
-    for pair in range(rows // PAIR):
-        start = pair * PAIR
-        dout = by_head(dout_ref[start : start + PAIR, :], width)
-        dprobs = dot(window(halo_ref, value_ref, pair), dout, NT)
-        probs = probs_ref[pair * WIN : (pair + 1) * WIN, :]
-        inner = jnp.sum(probs * dprobs, axis=0, keepdims=True)
-        dscores = probs * (dprobs - inner)
-        dscore_sum = dscores if dscore_sum is None else dscore_sum + dscores
-        dscores_ref[pair * WIN : (pair + 1) * WIN, :] = dscores.astype(jnp.bfloat16)
+    pairs = rows // PAIR
     key_of = lax.broadcasted_iota(jnp.int32, (PAIR, PAIR), 0)
     query_of = lax.broadcasted_iota(jnp.int32, (PAIR, PAIR), 1)
     after = query_of >= key_of
-    squares, tops = [], []
-    for h in range(heads):
-        lanes = slice(h * PAIR, (h + 1) * PAIR)
-        far, middle, near = (dscore_sum[b * PAIR : (b + 1) * PAIR, lanes] for b in range(3))
-        squares.append(jnp.where(after, 0.0, near))
-        squares.append(jnp.where(after, near, middle))
-        tops.append(jnp.sum(far + jnp.where(after, middle, 0.0), axis=0, keepdims=True))
-    sums = diagonals(squares)
     last = lax.broadcasted_iota(jnp.int32, (1, PAIR), 1) == PAIR - 1
-    pos = [s + jnp.where(last, jnp.sum(t, axis=1, keepdims=True), 0.0) for s, t in zip(sums[1::2], tops)]
-    by_rank = by_owner(sums[0::2], pos)
+    douts = [by_head(dout_ref[p * PAIR : (p + 1) * PAIR, :], width) for p in range(pairs)]
+    values = [window(halo_ref, value_ref, p) for p in range(pairs)]
+    neg, pos = [], []
+    for first in range(0, heads, 2):
+        dprobs = [dot(values[p], douts[p][first * PAIR : (first + 2) * PAIR], NT) for p in range(pairs)]
+        for head in (first, first + 1):
+            lanes = slice(head * PAIR, (head + 1) * PAIR)
+            mine = [d[:, (head - first) * PAIR : (head - first + 1) * PAIR] for d in dprobs]
+            inner = [
+                jnp.sum(probs_ref[p * WIN : (p + 1) * WIN, lanes] * mine[p], axis=0, keepdims=True) for p in range(pairs)
+            ]
+            blocks = []
+            for b in range(WIN // PAIR):
+                total = None
+                for p in range(pairs):
+                    at = slice(p * WIN + b * PAIR, p * WIN + (b + 1) * PAIR)
+                    dscores = probs_ref[at, lanes] * (mine[p][b * PAIR : (b + 1) * PAIR] - inner[p])
+                    dscores_ref[at, lanes] = dscores.astype(jnp.bfloat16)
+                    total = dscores if total is None else total + dscores
+                blocks.append(total)
+            far, middle, near = blocks
+            top = jnp.sum(far + jnp.where(after, middle, 0.0), axis=0, keepdims=True)
+            below, above = diagonals([jnp.where(after, 0.0, near), jnp.where(after, near, middle)])
+            neg.append(below)
+            pos.append(above + jnp.where(last, jnp.sum(top, axis=1, keepdims=True), 0.0))
+    by_rank = by_owner([jnp.concatenate([n, p], axis=1) for n, p in zip(neg, pos)])
     ranks = lax.axis_size("y")
     share = by_rank.shape[0] // ranks
     copies = table_ref.shape[0] // by_rank.shape[0]
@@ -134,18 +148,22 @@
         table_ref[y * share * copies : (y + 1) * share * copies, :] = block
 
 
-def by_owner(neg, pos):
-    heads = len(neg)
-    period = 2 * CLIP // lax.axis_size("z")
-    rows = lax.broadcasted_iota(jnp.int32, (period, CLIP), 0)
-    mine = lax.broadcasted_iota(jnp.int32, (period, CLIP), 1) % period == rows
-    spread = jnp.concatenate([jnp.where(mine, row, 0.0) for row in neg + pos], axis=1)
-    source = lax.broadcasted_iota(jnp.int32, (2 * heads * CLIP, PAIR), 0)
-    lane = lax.broadcasted_iota(jnp.int32, (2 * heads * CLIP, PAIR), 1)
-    head = source // CLIP % heads
-    index = source % CLIP + source // (heads * CLIP) * CLIP
-    place = jnp.where(lane == index // period * heads + head, 1.0, 0.0)
-    return dot(spread, place, NN, precision=HIGHEST)
+def by_owner(columns):
+    heads, table_rows = len(columns), 2 * CLIP
+    period = table_rows // lax.axis_size("z")
+    iota = partial(lax.broadcasted_iota, jnp.int32)
+    mine = iota((period, table_rows), 1) % period == iota((period, table_rows), 0)
+    spread = jnp.concatenate([jnp.where(mine, column, 0.0) for column in columns], axis=0)
+    rank = iota((table_rows, PAIR), 0) // period
+    place = jnp.where(iota((table_rows, PAIR), 1) // heads == rank, 1.0, 0.0).astype(jnp.bfloat16)
+    count = heads * period
+    found = dot(jnp.concatenate(thirds(spread), axis=0), place, NN)
+    found = found[:count] + found[count : 2 * count] + found[2 * count :]
+    head_of = iota((period, PAIR), 1) % heads
+    out = found[:period]
+    for h in range(1, heads):
+        out = jnp.where(head_of == h, found[h * period : (h + 1) * period], out)
+    return out
 
 
 def heads_kernel(heads, all_heads, terms_ref, out_ref):
@@ -155,16 +173,15 @@
     total = terms_ref[0:each, :]
     for y in range(1, lax.axis_size("y")):
         total = total + terms_ref[y * each : (y + 1) * each, :]
-    source = lax.broadcasted_iota(jnp.int32, (each, PAIR), 0)
-    lane = lax.broadcasted_iota(jnp.int32, (each, PAIR), 1)
+    iota = partial(lax.broadcasted_iota, jnp.int32)
+    source, lane = iota((each, PAIR), 0), iota((each, PAIR), 1)
     wanted = (lane // all_heads == source % share) & (lane % all_heads // heads == source // share)
-    spread = dot(total, jnp.where(wanted, 1.0, 0.0), TN, precision=HIGHEST)
-    source = lax.broadcasted_iota(jnp.int32, (PAIR, PAIR), 0)
-    lane = lax.broadcasted_iota(jnp.int32, (PAIR, PAIR), 1)
-    spread = jnp.where(source % heads == lane % heads, spread, 0.0)
-    rank = (lax.broadcasted_iota(jnp.int32, (ranks, PAIR), 0) + ranks // 2) % ranks
-    pick = lax.broadcasted_iota(jnp.int32, (ranks, PAIR), 1) // heads == rank
-    out_ref[...] = dot(jnp.where(pick, 1.0, 0.0), spread, NN, precision=HIGHEST)
+    place = jnp.where(wanted, 1.0, 0.0).astype(jnp.bfloat16)
+    spread = dot(jnp.concatenate(thirds(total), axis=0), jnp.concatenate([place] * 3, axis=0), TN)
+    spread = jnp.where(iota((PAIR, PAIR), 0) % heads == iota((PAIR, PAIR), 1) % heads, spread, 0.0)
+    rank = (iota((ranks, PAIR), 0) + ranks // 2) % ranks
+    pick = jnp.where(iota((ranks, PAIR), 1) // heads == rank, 1.0, 0.0).astype(jnp.bfloat16)
+    out_ref[...] = dot(jnp.concatenate([pick] * 3, axis=1), jnp.concatenate(thirds(spread), axis=0), NN)
 
 
 def grads_kernel(

time: 72.8 us -> 72.1 us (level)
  transfers between devices with their start and end apart: 3 -> 3, of which waited for: 1 -> 1; matrix products, arithmetic and copies ran while one was open for 1% -> 1% of each run, Pallas kernels for 3% -> 2%
where the time goes in v4:
time: 72.1 us; the launch traced here: 71.8 us
  blocking collectives  55.4 us (77%)
  starting transfers between devices  8.51 us (12%)
  Pallas kernels  5.42 us (8%)
  local copies, waits for them, and re-layouts  0.88 us (1%)
  waiting for transfers between devices  0.86 us (1%)
  between operations  0.74 us (1%)
    all_to_all x1, blocking collectives, shards(): lax.all_to_all(table.reshape(ranks, 1, PAIR), 'z', 0, 0, axis_index_group...  31.8 us
    all_to_all x1, blocking collectives, shards(): lax.all_to_all(table.reshape(groups, share, PAIR), PLANE, 0, 0, tiled=True)  23.7 us
    ppermute x3, starting transfers between devices, passed_along(): lax.ppermute(block, SP, [(i - distance, i) for i in devices if i - distan...  8.51 us
    pallas_call x1, Pallas kernels, shards(): kernel(grads_kernel, outs, 4000000000)  1.52 us
  transfers between devices with their start and end apart: 3, of which 1 were waited for; matrix products, arithmetic and copies ran while one was open for 1% of the time, Pallas kernels for 2%

profile of v4, /device:TPU:1, one launch (start us, length us, event | category | flops | bytes accessed | tf_op | source)
XLA Modules:
  0.0 71.8 jit_solution(8912887593697082442)
XLA Ops:
  0.6 4.0 %collective-permute-start.1 = (bf16[256,256]{1,0:T(8,128)(2,1)}, bf16[256,256]{1,0:T(8,128)(2,1)S(1)}, u32[]{:S(2)}, u32[]{:S(2)}) collective-permute-start(bf16[256,256]{1,0:T(8,128)(2,1)} %value_ref.1), channel_id=1, source_target_pairs={{0,8},{8,16},{16,24},{24,32},{32,40},{40,48},{48,56},{56,64},{64,7... | collective-permute-start | bytes 393224 | tf_op jit(solution)/shard_map/ppermute | solution.py:241
  4.7 3.2 %collective-permute-start = (bf16[256,256]{1,0:T(8,128)(2,1)}, bf16[256,256]{1,0:T(8,128)(2,1)S(1)}, u32[]{:S(2)}, u32[]{:S(2)}) collective-permute-start(bf16[256,256]{1,0:T(8,128)(2,1)} %key_ref.3), channel_id=1, source_target_pairs={{0,8},{8,16},{16,24},{24,32},{32,40},{40,48},{48,56},{56,64},{64,7... | collective-permute-start | bytes 393224 | tf_op jit(solution)/shard_map/ppermute | solution.py:241
  7.9 0.9 %copy.10.table_ref = f32[256,32]{1,0:T(8,128)S(1)} copy(f32[256,32]{0,1:T(8,128)} %param.9) | data formatting | bytes 65536 | tf_op args[4]
  8.7 0.0 copy-start.1
  8.7 0.0 copy-start.2
  8.8 0.5 shard_map.84.bias_ref
  9.2 0.0 copy-start
  9.3 0.0 copy-start.3
  9.3 0.9 %collective-permute-done.halo_ref = bf16[256,256]{1,0:T(8,128)(2,1)S(1)} collective-permute-done((bf16[256,256]{1,0:T(8,128)(2,1)}, bf16[256,256]{1,0:T(8,128)(2,1)S(1)}, u32[]{:S(2)}, u32[]{:S(2)}) %collective-permute-start) | collective-permute-done | bytes 131104 | tf_op jit(solution)/shard_map/ppermute | solution.py:241
  10.1 0.0 copy-done.1
  10.1 0.0 copy-done.2
  10.1 0.9 %shard_map.85 = (f32[768,512]{1,0:T(8,128)S(1)}, bf16[768,512]{1,0:T(8,128)(2,1)S(1)}) custom-call(bf16[256,256]{1,0:T(8,128)(2,1)S(1)} %copy-done.1, bf16[256,256]{1,0:T(8,128)(2,1)S(1)} %copy-done.2, bf16[256,256]{1,0:T(8,128)(2,1)S(1)} %collective-permute-done.halo_ref, f32[384,512]{1,0:T(8,128)S(1)} %shard_map.84.bias_ref), custom_call_target="tpu_custom_call" | custom-call | flops 4000000000 | bytes 2000000 | tf_op jit(solution)/shard_map/pallas_call | solution.py:269
  11.1 0.0 collective-permute-done.1.halo_ref
  11.1 0.0 copy-done
  11.1 0.0 copy-done.3
  11.1 1.4 %shard_map.86 = (bf16[768,512]{1,0:T(8,128)(2,1)S(1)}, f32[64,128]{1,0:T(8,128)S(1)}) custom-call(bf16[256,256]{1,0:T(8,128)(2,1)S(1)} %copy-done, bf16[256,256]{1,0:T(8,128)(2,1)S(1)} %copy-done.3, bf16[256,256]{1,0:T(8,128)(2,1)S(1)} %collective-permute-done.1.halo_ref, f32[768,512]{1,0:T(8,128)S(1)} %get-tuple-element.15.probs_ref), custom_call_target="tpu_custom_call" | custom-call | flops 4000000000 | bytes 2000000 | tf_op jit(solution)/shard_map/pallas_call | solution.py:273
  12.5 1.5 %shard_map.87 = (bf16[256,256]{1,0:T(8,128)(2,1)}, f32[512,256]{1,0:T(8,128)S(1)}, bf16[512,256]{1,0:T(8,128)(2,1)S(1)}) custom-call(bf16[256,256]{1,0:T(8,128)(2,1)S(1)} %copy-done.1, bf16[256,256]{1,0:T(8,128)(2,1)S(1)} %copy-done.2, bf16[256,256]{1,0:T(8,128)(2,1)S(1)} %copy-done.3, bf16[256,256]{1,0:T(8,128)(2,1)S(1)} %collective-permute-done.halo_ref, ...), custom_call_target="tpu_custom_call" | custom-call | flops 4000000000 | bytes 2000000 | tf_op jit(solution)/shard_map/pallas_call | solution.py:276
  14.0 1.3 %collective-permute-start.2 = (bf16[512,256]{1,0:T(8,128)(2,1)S(1)}, bf16[512,256]{1,0:T(8,128)(2,1)S(1)}, u32[]{:S(2)}, u32[]{:S(2)}) collective-permute-start(bf16[512,256]{1,0:T(8,128)(2,1)S(1)} %get-tuple-element.19), channel_id=1, source_target_pairs={{8,0},{16,8},{24,16},{32,24},{40,32},{48,40},{56,48},{64,56},{72,6... | collective-permute-start | bytes 786440 | tf_op jit(solution)/shard_map/ppermute | solution.py:241
  15.3 23.7 %all_to_all.10 = f32[32,2,128]{2,1,0:T(2,128)S(1)} all-to-all(f32[32,2,128]{2,1,0:T(2,128)S(1)} %bitcast.6), channel_id=1, replica_groups=mesh['z'=32,'y'=4,'tp'=8] {'y','tp'}, dimensions={0} | all-to-all | bytes 65536 | tf_op jit(solution)/shard_map/all_to_all | solution.py:274
  39.0 0.3 shard_map.88
  39.3 31.8 %all_to_all.11 = f32[32,1,128]{2,1,0:T(1,128)S(1)} all-to-all(f32[32,1,128]{2,1,0:T(1,128)S(1)} %bitcast.9), channel_id=1, replica_groups={{512,544,576,608,640,672,704,736,768,800,832,864,896,928,960,992,0,32,6..., dimensions={0} | all-to-all | bytes 32768 | tf_op jit(solution)/shard_map/all_to_all | solution.py:284
  71.1 0.0 collective-permute-done.2.arrived_ref
  71.1 0.8 %shard_map.89 = (bf16[256,256]{1,0:T(8,128)(2,1)}, bf16[256,256]{1,0:T(8,128)(2,1)}, f32[2,32]{1,0:T(2,128)}) custom-call(f32[512,256]{1,0:T(8,128)S(1)} %get-tuple-element.18.own_ref, bf16[512,256]{1,0:T(8,128)(2,1)S(1)} %collective-permute-done.2.arrived_ref, f32[32,128]{1,0:T(8,128)S(1)} %bitcast.8), custom_call_target="tpu_custom_call" | custom-call | flops 500000000 | bytes 2000000 | tf_op jit(solution)/shard_map/pallas_call | solution.py:286
Async XLA Ops:
  0.6 10.4 %collective-permute-start.1 = (bf16[256,256]{1,0:T(8,128)(2,1)}, bf16[256,256]{1,0:T(8,128)(2,1)S(1)}, u32[]{:S(2)}, u32[]{:S(2)}) collective-permute-start(bf16[256,256]{1,0:T(8,128)(2,1)} %value_ref.1), channel_id=1, source_target_pairs={{0,8},{8,16},{16,24},{24,32},{32,40},{40,48},{48,56},{56,64},{64,7... | collective-permute-start | bytes 393224 | tf_op jit(solution)/shard_map/ppermute | solution.py:241
  4.7 5.5 %collective-permute-start = (bf16[256,256]{1,0:T(8,128)(2,1)}, bf16[256,256]{1,0:T(8,128)(2,1)S(1)}, u32[]{:S(2)}, u32[]{:S(2)}) collective-permute-start(bf16[256,256]{1,0:T(8,128)(2,1)} %key_ref.3), channel_id=1, source_target_pairs={{0,8},{8,16},{16,24},{24,32},{32,40},{40,48},{48,56},{56,64},{64,7... | collective-permute-start | bytes 393224 | tf_op jit(solution)/shard_map/ppermute | solution.py:241
  8.7 1.4 %copy-start.1 = (bf16[256,256]{1,0:T(8,128)(2,1)S(1)}, bf16[256,256]{1,0:T(8,128)(2,1)}, u32[]{:S(2)}) copy-start(bf16[256,256]{1,0:T(8,128)(2,1)} %query_ref.3) | copy-start | bytes 393220
  8.7 1.4 %copy-start.2 = (bf16[256,256]{1,0:T(8,128)(2,1)S(1)}, bf16[256,256]{1,0:T(8,128)(2,1)}, u32[]{:S(2)}) copy-start(bf16[256,256]{1,0:T(8,128)(2,1)} %key_ref.3) | copy-start | bytes 393220
  9.2 1.9 %copy-start = (bf16[256,256]{1,0:T(8,128)(2,1)S(1)}, bf16[256,256]{1,0:T(8,128)(2,1)}, u32[]{:S(2)}) copy-start(bf16[256,256]{1,0:T(8,128)(2,1)} %value_ref.1) | copy-start | bytes 393220
  9.3 1.8 %copy-start.3 = (bf16[256,256]{1,0:T(8,128)(2,1)S(1)}, bf16[256,256]{1,0:T(8,128)(2,1)}, u32[]{:S(2)}) copy-start(bf16[256,256]{1,0:T(8,128)(2,1)} %dout_ref.3) | copy-start | bytes 393220
  14.0 57.0 %collective-permute-start.2 = (bf16[512,256]{1,0:T(8,128)(2,1)S(1)}, bf16[512,256]{1,0:T(8,128)(2,1)S(1)}, u32[]{:S(2)}, u32[]{:S(2)}) collective-permute-start(bf16[512,256]{1,0:T(8,128)(2,1)S(1)} %get-tuple-element.19), channel_id=1, source_target_pairs={{8,0},{16,8},{24,16},{32,24},{40,32},{48,40},{56,48},{64,56},{72,6... | collective-permute-start | bytes 786440 | tf_op jit(solution)/shard_map/ppermute | solution.py:241
